TPU v7x, 512 devices: a whole 4x4x16 slice. The times are simulated.
512 devices in a mesh: gr: 2 (over z_hi), fs: 32 (over z_lo, y), tp: 8 (over x, core).
Axes of the slice: x: 4, y: 4, z: 16 (z_hi: 2, z_lo: 8; z = z_hi * 8 + z_lo), core: 2. Of those that a mesh axis runs over, the one named last changes fastest.
Arguments:
- tokens: bfloat16 [8192, 2048], P(('gr', 'tp')), may hold values from -6 to 6
- norm_gain: float32 [2048], P('fs'), may hold values from 0.1 to 1.9
- up_weight: float32 [2048, 8192], P('fs', ('gr', 'tp')), may hold values from -0.125 to 0.125
- down_weight: float32 [8192, 2048], P('fs', ('gr', 'tp')), may hold values from -0.125 to 0.125
Outputs:
- sampler_up: bfloat16 [2048, 8192], P(None, 'fs')
- sampler_down: bfloat16 [8192, 2048], P('fs')
- mixed: bfloat16 [8192, 2048], P(('gr', 'tp'), 'fs')
All inputs are finite; a program needn't handle non-finite values.
Results may differ from a plain program's by a relative error of at most 0.023.
Values may be sent and summed in bfloat16 or wider, within the bound.
A program may use at most 64 MiB of HBM per device.

v0:
```python
import jax
import jax.numpy as jnp
from jax import lax
from jax.sharding import PartitionSpec as P


def laid_out(parts, dim):
    lengths = list(parts.shape[1:])
    lengths[dim] *= parts.shape[0]
    return jnp.moveaxis(parts, 0, dim).reshape(lengths)


def one_gather(arrays, axis, dims):
    vector = jnp.concatenate([a.reshape(-1) for a in arrays])
    lines, at, done = (lax.all_gather(vector, axis), 0, [])
    for a, dim in zip(arrays, dims):
        parts = lines[:, at : at + a.size].reshape(-1, *a.shape)
        done.append(laid_out(parts, dim))
        at += a.size
    return tuple(done)


def split_up(x, dim, count):
    before, after = (x.shape[:dim], x.shape[dim + 1 :])
    return jnp.moveaxis(x.reshape(*before, count, -1, *after), dim, 0)


def sent_and_summed(x, axis, dim):
    parts = split_up(x, dim, lax.axis_size(axis))
    arrived = lax.all_to_all(parts, axis, split_axis=0, concat_axis=0, tiled=True)
    return arrived.astype(jnp.float32).sum(axis=0)


def per_device(tokens, norm_gain, up_weight, down_weight):
    up_scaled = (norm_gain[:, None] * up_weight).astype(jnp.bfloat16)
    down_half = down_weight.astype(jnp.bfloat16)
    up_columns, down_columns = one_gather((up_scaled, down_half), ("gr", "tp"), (1, 1))
    up_block = lax.all_to_all(up_columns, "fs", split_axis=1, concat_axis=0, tiled=True)
    widened = tokens.astype(jnp.float32)
    normed = (
        widened * lax.rsqrt(jnp.mean(widened * widened, axis=-1, keepdims=True) + 1e-06)
    ).astype(jnp.bfloat16)
    preact = jnp.dot(normed, up_block, preferred_element_type=jnp.float32)
    hidden = jnp.square(jax.nn.relu(preact)).astype(jnp.bfloat16)
    summed = sent_and_summed(
        lax.dot_general(
            down_columns, hidden, (((0,), (1,)), ((), ())), preferred_element_type=jnp.float32
        ).astype(jnp.bfloat16),
        "fs",
        0,
    )
    mixed = summed.astype(jnp.bfloat16).T
    return (up_block, down_columns, mixed)


def solution(mesh):
    in_specs = (P(("gr", "tp"), None), P("fs"), P("fs", ("gr", "tp")), P("fs", ("gr", "tp")))
    out_specs = (P(None, "fs"), P("fs", None), P(("gr", "tp"), "fs"))
    return jax.shard_map(
        per_device, mesh=mesh, in_specs=in_specs, out_specs=out_specs, check_vma=False
    )
```

profile of v0, /device:TPU:1, one launch (start us, length us, event | category | flops | bytes accessed | tf_op | source)
XLA Modules:
  0.0 286.5 jit_solution(4625341958029918744)
XLA Ops:
  7.2 0.0 all-gather.3.cloned.1.call-start
  7.2 1.0 fusion.17
  8.2 0.9 convert_bitcast_fusion
  9.2 0.7 pad_maximum_fusion
  9.8 0.0 all-gather.3.cloned.1.call-update
  9.8 99.7 %all-gather.3.cloned.1.call-done = bf16[1048576]{0:T(1024)(128)(2,1)} async-done(((bf16[65536]{0:T(1024)(128)(2,1)}), bf16[1048576]{0:T(1024)(128)(2,1)}) %all-gather.3.cloned.1.call-update) | async-done | bytes 2097168 | tf_op jit(solution)/shard_map/all_gather | solution.py:15
  109.6 2.1 reshape.44
  111.7 1.1 slice_bitcast_fusion
  112.8 0.1 copy.20
  113.0 0.4 all_to_all.17
  113.4 1.6 copy.13
  114.9 5.0 %all-to-all-start = ((bf16[64,32,256]{2,0,1:T(8,128)(2,1)}), bf16[64,32,256]{2,0,1:T(8,128)(2,1)S(1)}, u32[]{:S(2)}, u32[]{:S(2)}) async-start(bf16[64,32,256]{2,0,1:T(8,128)(2,1)} %copy.13), calls=%async_computation | async-start | bytes 2097152 | tf_op jit(solution)/shard_map/all_to_all | solution.py:38
  119.9 2.1 fusion
  122.0 0.0 copy-done.1
  122.0 0.2 copy.18
  122.2 0.5 copy.14
  122.7 0.0 copy-start
  122.7 47.3 %all-to-all-done = bf16[64,32,256]{2,0,1:T(8,128)(2,1)S(1)} async-done(((bf16[64,32,256]{2,0,1:T(8,128)(2,1)}), bf16[64,32,256]{2,0,1:T(8,128)(2,1)S(1)}, u32[]{:S(2)}, u32[]{:S(2)}) %all-to-all-start) | async-done | bytes 1048608 | tf_op jit(solution)/shard_map/all_to_all | solution.py:38
  170.0 5.3 %convolution_convert_fusion = bf16[2048,512]{1,0:T(8,128)(2,1)} fusion(bf16[256,2048]{0,1:T(8,128)(2,1)S(1)} %bitcast.27, bf16[2048,256]{1,0:T(8,128)(2,1)S(1)} %bitcast.25, bf16[512,2048]{1,0:T(8,128)(2,1)} %param.4, f32[512]{0:T(512)S(1)} %add_rsqrt_fusion), kind=kOutput, calls=%fused_computation.4 | convolution fusion | flops 1078329344 | bytes 6293504 | tf_op jit(solution)/shard_map/dot_general | solution.py:46
  175.3 7.8 %all-to-all-start.1 = ((bf16[32,64,512]{2,1,0:T(8,128)(2,1)}), bf16[32,64,512]{2,1,0:T(8,128)(2,1)S(1)}, u32[]{:S(2)}, u32[]{:S(2)}) async-start(bf16[32,64,512]{2,1,0:T(8,128)(2,1)} %bitcast.32), calls=%async_computation.1 | async-start | bytes 4194304 | tf_op jit(solution)/shard_map/all_to_all | solution.py:30
  183.1 2.3 copy.15
  185.3 92.4 %all-to-all-done.1 = bf16[32,64,512]{2,1,0:T(8,128)(2,1)S(1)} async-done(((bf16[32,64,512]{2,1,0:T(8,128)(2,1)}), bf16[32,64,512]{2,1,0:T(8,128)(2,1)S(1)}, u32[]{:S(2)}, u32[]{:S(2)}) %all-to-all-start.1) | async-done | bytes 2097184 | tf_op jit(solution)/shard_map/all_to_all | solution.py:30
  277.7 0.9 reduce_sum.22
  278.7 1.0 copy.22
  (4 shorter events, 0.0 us)
Async XLA Ops:
  7.2 102.4 %all-gather.3.cloned.1.call-start = ((), (), s32[]{:S(2)}) async-start(), calls=%async_computation.2 | async-start | bytes 2228224 | tf_op jit(solution)/shard_map/all_gather | solution.py:15
  114.9 7.1 %copy-start.1 = (bf16[2,8,256,128]{3,1,2,0:T(8,128)(2,1)S(1)}, bf16[2,8,256,128]{3,1,2,0:T(8,128)(2,1)}, u32[]{:S(2)}) copy-start(bf16[2,8,256,128]{3,1,2,0:T(8,128)(2,1)} %get-tuple-element.9) | copy-start | bytes 3145732
  114.9 55.1 %all-to-all-start = ((bf16[64,32,256]{2,0,1:T(8,128)(2,1)}), bf16[64,32,256]{2,0,1:T(8,128)(2,1)S(1)}, u32[]{:S(2)}, u32[]{:S(2)}) async-start(bf16[64,32,256]{2,0,1:T(8,128)(2,1)} %copy.13), calls=%async_computation | async-start | bytes 2097152 | tf_op jit(solution)/shard_map/all_to_all | solution.py:38
  122.7 52.6 %copy-start = (bf16[256,16,128]{0,2,1:T(8,128)(2,1)}, bf16[256,16,128]{0,2,1:T(8,128)(2,1)S(1)}, u32[]{:S(2)}) copy-start(bf16[256,16,128]{0,2,1:T(8,128)(2,1)S(1)} %copy.14) | copy-start | bytes 3145732
  175.3 102.4 %all-to-all-start.1 = ((bf16[32,64,512]{2,1,0:T(8,128)(2,1)}), bf16[32,64,512]{2,1,0:T(8,128)(2,1)S(1)}, u32[]{:S(2)}, u32[]{:S(2)}) async-start(bf16[32,64,512]{2,1,0:T(8,128)(2,1)} %bitcast.32), calls=%async_computation.1 | async-start | bytes 4194304 | tf_op jit(solution)/shard_map/all_to_all | solution.py:30
Sparse Core Ops, SparseCore 0:
  11.9 97.6 all-gather.2
where the time goes:
time: 287 us; the launch traced here: 286 us
  waiting for transfers between devices  239 us (83%)
  between operations  14.1 us (5%)
  starting transfers between devices  12.8 us (4%)
  local copies, waits for them, and re-layouts  9.32 us (3%)
  other arithmetic  5.57 us (2%)
  matrix products  5.31 us (2%)
    all_gather x1, waiting for transfers between devices, one_gather(): lines, at, done = (lax.all_gather(vector, axis), 0, [])  99.7 us
    all_to_all x1, waiting for transfers between devices, sent_and_summed(): lax.all_to_all(parts, axis, split_axis=0, concat_axis=0, tiled=True)  92.4 us
    all_to_all x1, waiting for transfers between devices, per_device(): lax.all_to_all(up_columns, 'fs', split_axis=1, concat_axis=0, tiled=True)  47.3 us
    all_to_all x1, starting transfers between devices, sent_and_summed(): lax.all_to_all(parts, axis, split_axis=0, concat_axis=0, tiled=True)  7.76 us
  transfers between devices with their start and end apart: 3, of which 3 were waited for; matrix products, arithmetic and copies ran while one was open for 2% of the time, Pallas kernels for 0%

commit v1 on v0

v1 whole, which is shorter than its diff:
```python
import functools

import jax
import jax.numpy as jnp
from jax import lax
from jax.experimental import pallas as pl
from jax.experimental.pallas import tpu as pltpu
from jax.sharding import PartitionSpec as P

MESH = pl.DeviceIdType.MESH
F32 = jnp.float32
BF16 = jnp.bfloat16

TOK = 512
D = 2048
UNITS = 256
NT = 2
TC = TOK // NT

UP1 = 0
UPX1 = 4
UPX2 = 8
UPC = 10
DNG = 18
DNX1 = 19
DNX2 = 23
DNC = 25
DTY = 33
DTX1 = 37
DTX2 = 39
DTC = 41
HY1 = 46
HY2 = HY1 + 2 * NT
RS = HY2 + 2 * NT
N_MSG = RS + 3 * NT


def kernel(
    tok_hbm, gain_ref, upw_ref, dnw_ref,
    up_out, dn_out, mix_ref,
    u_send, up_buf, dn_buf, dt_send, dt_buf, nrm, h_buf,
    s1, r1, k1, s2, r2, k2, s3, r3, k3,
    ssem, rsem, lsem,
):
    g = lax.axis_index("gr")
    f = lax.axis_index("fs")
    t = lax.axis_index("tp")
    zl, y = f // 4, f % 4
    x, k = t // 2, t % 2
    ok = 1 - k
    og = 1 - g

    def dev(gg, zz, yy, xx, kk):
        return (gg, zz * 4 + yy, xx * 2 + kk)

    def send(src, dst, i, to, j=None):
        copy = pltpu.make_async_remote_copy(
            src_ref=src, dst_ref=dst,
            send_sem=ssem.at[i], recv_sem=rsem.at[i if j is None else j],
            device_id=to, device_id_type=MESH,
        )
        copy.start()
        return copy

    def arrived(dst, i):
        pltpu.make_async_remote_copy(
            src_ref=dst, dst_ref=dst,
            send_sem=ssem.at[0], recv_sem=rsem.at[i],
            device_id=dev(g, zl, y, x, ok), device_id_type=MESH,
        ).wait_recv()

    right, left, far = (x + 1) % 4, (x + 3) % 4, (x + 2) % 4
    to_right, to_left = dev(g, zl, y, right, k), dev(g, zl, y, left, k)
    to_core = dev(g, zl, y, x, ok)
    y_up, y_down, y_far = (y + 1) % 4, (y + 3) % 4, (y + 2) % 4
    to_yup, to_ydown = dev(g, zl, y_up, x, k), dev(g, zl, y_down, x, k)
    b0, b1, b2 = zl % 2, (zl // 2) % 2, zl // 4
    z1 = zl + 1 - 2 * b0
    z2 = zl + 2 - 4 * b1
    z4 = zl + 4 - 8 * b2

    xs, ks, hs = zl % 4, y // 2, y % 2

    def a_of(xx):
        return (xx - xs - hs - 2 * g + 8) % 4

    a_me = a_of(x)
    sources = [
        (q * 2 + w, dev(b2, a_me + 4 * q, 2 * ok + w, xs, ks)) for q in range(2) for w in range(2)
    ]

    barrier = pltpu.get_barrier_semaphore()
    greet = [s for _, s in sources] + [
        dev(og, zl, y, x, k), to_right, to_left, to_core,
        to_yup, to_ydown, dev(g, zl, y_far, x, k),
        dev(g, z1, y, x, k), dev(g, z2, y, x, k), dev(g, z4, y, x, k),
    ]
    for who in greet:
        pl.semaphore_signal(barrier, inc=1, device_id=who, device_id_type=MESH)

    tok_copy = pltpu.make_async_copy(tok_hbm, nrm, lsem.at[0])
    tok_copy.start()

    rows = lax.broadcasted_iota(jnp.int32, (64, 64), 0)
    cols = lax.broadcasted_iota(jnp.int32, (64, 64), 1)
    gain_wide = jnp.broadcast_to(gain_ref[...], (64, 64))
    gain = jnp.sum(jnp.where(rows == cols, gain_wide, 0.0), axis=1, keepdims=True)
    for h in range(2):
        u_send[h] = (gain * upw_ref[:, h * 256 : (h + 1) * 256]).astype(BF16)

    def dn_cols(gg, xx, kk):
        return pl.ds(pl.multiple_of((gg * 8 + xx * 2 + kk) * 128, 128), 128)

    def dn_piece(gg, xx, kk):
        return dn_buf.at[:, dn_cols(gg, xx, kk)]

    dn_mine = dnw_ref[...]
    dn_buf[:, dn_cols(g, x, k)] = dn_mine.astype(BF16)

    pl.semaphore_wait(barrier, len(greet))

    def up_piece(xx, q, kk):
        start = ((a_of(xx) + 4 * q) * 4 + 2 * (1 - kk)) * 64
        return up_buf.at[pl.ds(pl.multiple_of(start, 128), 128), :]

    sent = []
    j_me = (zl // 4) * 2 + y % 2
    for gg in range(2):
        for h in range(2):
            xx = (x + zl + h + 2 * gg) % 4
            to = (gg, (4 * g + x) * 4 + 2 * k + h, xx * 2 + (1 - y // 2))
            slot = up_buf.at[pl.ds(pl.multiple_of(f * 64, 64), 64), :]
            sent.append(send(u_send.at[h], slot, UP1 + gg * 2 + h, to, UP1 + j_me))
    sent.append(send(dn_piece(g, x, k), dn_piece(g, x, k), DNG, dev(og, zl, y, x, k)))

    dt_mine = dn_mine.T.astype(BF16)
    for h in range(2):
        dt_send[h, pl.ds(pl.multiple_of(g * 64, 64), 64), :] = dt_mine[h * 64 : (h + 1) * 64]

    tok_copy.wait()

    def norm_rows(i, _):
        at = pl.ds(pl.multiple_of(i * 16, 16), 16)
        wide = nrm[at, :].astype(F32)
        scale = lax.rsqrt(jnp.mean(wide * wide, axis=-1, keepdims=True) + 1e-06)
        nrm[at, :] = (wide * scale).astype(BF16)
        return 0

    lax.fori_loop(0, TOK // 16, norm_rows, 0)

    for j, _ in sources:
        q, w = j // 2, j % 2
        start = ((a_me + 4 * q) * 4 + 2 * ok + w) * 64
        arrived(up_buf.at[pl.ds(pl.multiple_of(start, 64), 64), :], UP1 + j)
        if w == 1:
            piece = up_piece(x, q, k)
            sent.append(send(piece, piece, UPX1 + q, to_right))
            sent.append(send(piece, piece, UPX1 + 2 + q, to_left))
            sent.append(send(piece, piece, UPC + q, to_core))

    arrived(dn_piece(og, x, k), DNG)
    for q in range(2):
        piece = dn_piece(q, x, k)
        sent.append(send(piece, piece, DNX1 + q, to_right))
        sent.append(send(piece, piece, DNX1 + 2 + q, to_left))
        sent.append(send(piece, piece, DNC + q, to_core))

    def dt_rows(xx, start=0, size=128):
        at = ((xx % 2) * 4 + (xx // 2) * 2) * 64 + start
        return pl.ds(pl.multiple_of(at, 64), size)

    dt_other = dn_buf[:, dn_cols(og, x, k)].astype(F32).T.astype(BF16)
    for h in range(2):
        dt_send[h, pl.ds(pl.multiple_of(og * 64, 64), 64), :] = dt_other[h * 64 : (h + 1) * 64]
    for h in range(2):
        target = 2 * k + h

        def dt_copy(h=h, target=target):
            return pltpu.make_async_remote_copy(
                src_ref=dt_send.at[h], dst_ref=dt_buf.at[y, dt_rows(x), :],
                send_sem=ssem.at[DTY + h], recv_sem=rsem.at[DTY + y],
                device_id=dev(g, zl, target, x, k), device_id_type=MESH,
            )

        @pl.when(target != y)
        def _():
            dt_copy().start()

        @pl.when(target == y)
        def _():
            dt_buf[y, dt_rows(x), :] = dt_send[h]

    for q in range(2):
        piece = up_piece(left, q, k)
        arrived(piece, UPX1 + q)
        if q == 0:
            sent.append(send(piece, piece, UPX2, to_right))
        sent.append(send(piece, piece, UPC + 2 + q, to_core))
        piece = up_piece(right, q, k)
        arrived(piece, UPX1 + 2 + q)
        if q == 1:
            sent.append(send(piece, piece, UPX2 + 1, to_left))
        sent.append(send(piece, piece, UPC + 4 + q, to_core))
    for q in range(2):
        piece = up_piece(far, q, k)
        arrived(piece, UPX2 + q)
        sent.append(send(piece, piece, UPC + 6 + q, to_core))

    def dn_forward():
        for q in range(2):
            piece = dn_piece(q, left, k)
            arrived(piece, DNX1 + q)
            if q == 0:
                sent.append(send(piece, piece, DNX2, to_right))
            sent.append(send(piece, piece, DNC + 2 + q, to_core))
            piece = dn_piece(q, right, k)
            arrived(piece, DNX1 + 2 + q)
            if q == 1:
                sent.append(send(piece, piece, DNX2 + 1, to_left))
            sent.append(send(piece, piece, DNC + 4 + q, to_core))

    dn_forward()

    owner = ks == k

    def dt_piece(xx, start=0, size=128):
        return dt_buf.at[:, dt_rows(xx, start, size), :]

    def dt_msg(piece, i, to):
        return pltpu.make_async_remote_copy(
            src_ref=piece, dst_ref=piece, send_sem=ssem.at[i], recv_sem=rsem.at[i],
            device_id=to, device_id_type=MESH,
        )

    @pl.when(owner)
    def _():
        for src in range(4):

            @pl.when(y != src)
            def _():
                arrived(dt_buf.at[src, dt_rows(x), :], DTY + src)

        dt_msg(dt_piece(x), DTX1, to_right).start()
        dt_msg(dt_piece(x), DTX1 + 1, to_left).start()
        dt_msg(dt_piece(x), DTC, to_core).start()

    for i, xx in enumerate((x, left, right, far)):
        for q in range(2):
            arrived(up_piece(xx, q, ok), UPC + 2 * i + q)
    up_copy = pltpu.make_async_copy(up_buf, up_out, lsem.at[1])
    up_copy.start()
    for j in range(NT):
        at = pl.ds(j * TC, TC)
        pre = jnp.dot(nrm[at, :], up_buf[...], preferred_element_type=F32)
        pre = jnp.maximum(pre, 0.0)
        h_buf[y, at, :] = (pre * pre).astype(BF16)
        piece = h_buf.at[y, at, :]
        sent.append(send(piece, piece, HY1 + 2 * j, to_yup))
        sent.append(send(piece, piece, HY1 + 2 * j + 1, to_ydown))

    @pl.when(owner)
    def _():
        arrived(dt_piece(left), DTX1)
        dt_msg(dt_piece(left, 0, 64), DTX2, to_right).start()
        dt_msg(dt_piece(left), DTC + 1, to_core).start()
        arrived(dt_piece(right), DTX1 + 1)
        dt_msg(dt_piece(right, 64, 64), DTX2 + 1, to_left).start()
        dt_msg(dt_piece(right), DTC + 2, to_core).start()

    for q in range(2):
        piece = dn_piece(q, far, k)
        arrived(piece, DNX2 + q)
        sent.append(send(piece, piece, DNC + 6 + q, to_core))

    half = TC // 2
    for j in range(NT):
        low, high = pl.ds(j * TC, half), pl.ds(j * TC + half, half)
        at = pl.ds(j * TC, TC)
        arrived(h_buf.at[y_down, at, :], HY1 + 2 * j)
        piece = h_buf.at[y_down, low, :]
        sent.append(send(piece, piece, HY2 + 2 * j, to_yup))
        arrived(h_buf.at[y_up, at, :], HY1 + 2 * j + 1)
        piece = h_buf.at[y_up, high, :]
        sent.append(send(piece, piece, HY2 + 2 * j + 1, to_ydown))

    @pl.when(owner)
    def _():
        for q in range(2):
            arrived(dt_piece(far, 64 * q, 64), DTX2 + q)
            dt_msg(dt_piece(far, 64 * q, 64), DTC + 3 + q, to_core).start()

    @pl.when(jnp.logical_not(owner))
    def _():
        arrived(dt_piece(x), DTC)
        arrived(dt_piece(left), DTC + 1)
        arrived(dt_piece(right), DTC + 2)
        for q in range(2):
            arrived(dt_piece(far, 64 * q, 64), DTC + 3 + q)

    def times_hidden(rows_at, size, at):
        total = jnp.zeros((size, TC), F32)
        for yy in range(4):
            total += lax.dot_general(
                dt_buf[yy, rows_at, :], h_buf[yy, at, :],
                (((1,), (1,)), ((), ())), preferred_element_type=F32,
            )
        return total

    def aligned(start, size):
        return pl.ds(pl.multiple_of(start, 64), size)

    to_z1, to_z2, to_z4 = (dev(g, zz, y, x, k) for zz in (z1, z2, z4))
    for j in range(NT):
        at = pl.ds(j * TC, TC)
        low, high = pl.ds(j * TC, half), pl.ds(j * TC + half, half)
        arrived(h_buf.at[y_far, low, :], HY2 + 2 * j)
        arrived(h_buf.at[y_far, high, :], HY2 + 2 * j + 1)
        s1[j] = times_hidden(aligned((1 - b0) * 256, 256), 256, at).astype(BF16)
        sent.append(send(s1.at[j], r1.at[j], RS + 3 * j, to_z1))
        k1[j] = times_hidden(aligned(b0 * 256, 256), 256, at)

    for j in range(NT):
        arrived(r1.at[j], RS + 3 * j)
        out, keep = aligned((1 - b1) * 128, 128), aligned(b1 * 128, 128)
        s2[j] = (k1[j, out, :] + r1[j, out, :].astype(F32)).astype(BF16)
        sent.append(send(s2.at[j], r2.at[j], RS + 3 * j + 1, to_z2))
        k2[j] = k1[j, keep, :] + r1[j, keep, :].astype(F32)
    for j in range(NT):
        arrived(r2.at[j], RS + 3 * j + 1)
        out, keep = aligned((1 - b2) * 64, 64), aligned(b2 * 64, 64)
        s3[j] = (k2[j, out, :] + r2[j, out, :].astype(F32)).astype(BF16)
        sent.append(send(s3.at[j], r3.at[j], RS + 3 * j + 2, to_z4))
        k3[j] = k2[j, keep, :] + r2[j, keep, :].astype(F32)

    for i, xx in enumerate((x, left, right, far)):
        for q in range(2):
            arrived(dn_piece(q, xx, ok), DNC + 2 * i + q)
    dn_copy = pltpu.make_async_copy(dn_buf, dn_out, lsem.at[2])
    dn_copy.start()

    for j in range(NT):
        arrived(r3.at[j], RS + 3 * j + 2)
        mix_ref[:, j * TC : (j + 1) * TC] = (k3[j] + r3[j].astype(F32)).astype(BF16)

    for copy in sent:
        copy.wait_send()
    for h in range(2):

        @pl.when(2 * k + h != y)
        def _():
            pltpu.make_async_remote_copy(
                src_ref=dt_send.at[h], dst_ref=dt_send.at[h],
                send_sem=ssem.at[DTY + h], recv_sem=rsem.at[DTY],
                device_id=to_core, device_id_type=MESH,
            ).wait_send()

    @pl.when(owner)
    def _():
        dt_msg(dt_piece(x), DTX1, to_right).wait_send()
        dt_msg(dt_piece(x), DTX1 + 1, to_left).wait_send()
        dt_msg(dt_piece(x), DTC, to_core).wait_send()
        dt_msg(dt_piece(left, 0, 64), DTX2, to_right).wait_send()
        dt_msg(dt_piece(left), DTC + 1, to_core).wait_send()
        dt_msg(dt_piece(right, 64, 64), DTX2 + 1, to_left).wait_send()
        dt_msg(dt_piece(right), DTC + 2, to_core).wait_send()
        for q in range(2):
            dt_msg(dt_piece(far, 64 * q, 64), DTC + 3 + q, to_core).wait_send()

    up_copy.wait()
    dn_copy.wait()


def per_device(tokens, norm_gain, up_weight, down_weight):
    vmem = pl.BlockSpec(memory_space=pltpu.VMEM)
    anywhere = pl.BlockSpec(memory_space=pl.ANY)
    up_block, down_block, mixed = pl.pallas_call(
        kernel,
        out_shape=(
            jax.ShapeDtypeStruct((D, UNITS), BF16),
            jax.ShapeDtypeStruct((UNITS, D), BF16),
            jax.ShapeDtypeStruct((64, TOK), BF16),
        ),
        in_specs=[anywhere, vmem, vmem, vmem],
        out_specs=(anywhere, anywhere, vmem),
        scratch_shapes=[
            pltpu.VMEM((2, 64, 256), BF16),
            pltpu.VMEM((D, UNITS), BF16),
            pltpu.VMEM((UNITS, D), BF16),
            pltpu.VMEM((2, 128, 256), BF16),
            pltpu.VMEM((4, 512, 256), BF16),
            pltpu.VMEM((TOK, D), BF16),
            pltpu.VMEM((4, TOK, UNITS), BF16),
            pltpu.VMEM((NT, 256, TC), BF16),
            pltpu.VMEM((NT, 256, TC), BF16),
            pltpu.VMEM((NT, 256, TC), F32),
            pltpu.VMEM((NT, 128, TC), BF16),
            pltpu.VMEM((NT, 128, TC), BF16),
            pltpu.VMEM((NT, 128, TC), F32),
            pltpu.VMEM((NT, 64, TC), BF16),
            pltpu.VMEM((NT, 64, TC), BF16),
            pltpu.VMEM((NT, 64, TC), F32),
            pltpu.SemaphoreType.DMA((N_MSG,)),
            pltpu.SemaphoreType.DMA((N_MSG,)),
            pltpu.SemaphoreType.DMA((3,)),
        ],
        compiler_params=pltpu.CompilerParams(
            collective_id=0, has_side_effects=True, vmem_limit_bytes=40 * 1024 * 1024
        ),
        name="handoff",
    )(tokens, norm_gain.reshape(1, 64), up_weight, down_weight)
    return up_block, down_block, mixed.T


def solution(mesh):
    in_specs = (P(("gr", "tp"), None), P("fs"), P("fs", ("gr", "tp")), P("fs", ("gr", "tp")))
    out_specs = (P(None, "fs"), P("fs", None), P(("gr", "tp"), "fs"))
    return jax.shard_map(
        per_device, mesh=mesh, in_specs=in_specs, out_specs=out_specs, check_vma=False
    )
```

time: 287 us -> 86.6 us (0.30)
  the two profiles are of different devices: /device:TPU:1 before, /device:TPU:9 now
where the time goes in v1:
time: 86.6 us; the launch traced here: 86.4 us
  Pallas kernels  79.2 us (91%)
  local copies, waits for them, and re-layouts  6.62 us (8%)
    pallas_call x1, Pallas kernels, per_device(): pl.pallas_call(kernel, out_shape=(jax.ShapeDtypeStruct((D, UNITS), BF16),...  79.2 us
    unnamed x11, local copies, waits for them, and re-layouts  6.62 us

profile of v1, /device:TPU:9, one launch (start us, length us, event | category | flops | bytes accessed | tf_op | source)
XLA Modules:
  0.0 86.4 jit_solution(8660435002815187056)
XLA Ops:
  0.6 0.0 copy-start
  0.6 1.6 %copy-done = bf16[512,2048]{1,0:T(8,128)(2,1)S(1)} copy-done((bf16[512,2048]{1,0:T(8,128)(2,1)S(1)}, bf16[512,2048]{1,0:T(8,128)(2,1)}, u32[]{:S(2)}) %copy-start) | copy-done | bytes 2097176
  2.2 0.0 copy-start.1
  2.2 0.9 %copy-done.1 = f32[64,512]{1,0:T(8,128)S(1)} copy-done((f32[64,512]{1,0:T(8,128)S(1)}, f32[64,512]{1,0:T(8,128)}, u32[]{:S(2)}) %copy-start.1) | copy-done | bytes 131096
  3.1 0.0 copy-start.2
  3.1 0.9 %copy-done.2 = f32[256,128]{1,0:T(8,128)S(1)} copy-done((f32[256,128]{1,0:T(8,128)S(1)}, f32[256,128]{1,0:T(8,128)}, u32[]{:S(2)}) %copy-start.2) | copy-done | bytes 131096
  4.0 0.0 copy-start.3
  4.0 0.7 copy-done.3
  4.7 79.2 %handoff.1 = (bf16[2048,256]{1,0:T(8,128)(2,1)S(1)}, bf16[256,2048]{1,0:T(8,128)(2,1)S(1)}, bf16[64,512]{1,0:T(8,128)(2,1)S(1)}) custom-call(bf16[512,2048]{1,0:T(8,128)(2,1)S(1)} %copy-done, f32[1,64]{1,0:T(1,128)S(1)} %bitcast.3, f32[64,512]{1,0:T(8,128)S(1)} %copy-done.1, f32[256,128]{1,0:T(8,128)S(1)} %copy-done.2), custom_call_target="tpu_custom_call" | custom-call | tf_op jit(solution)/shard_map/handoff/pallas_call | solution.py:376
  83.9 1.0 %copy.10 = bf16[2048,256]{1,0:T(8,128)(2,1)} copy(bf16[2048,256]{1,0:T(8,128)(2,1)S(1)} %get-tuple-element.12) | data formatting | bytes 2097152
  84.8 1.0 %copy.11 = bf16[256,2048]{1,0:T(8,128)(2,1)} copy(bf16[256,2048]{1,0:T(8,128)(2,1)S(1)} %get-tuple-element.13) | data formatting | bytes 2097152
  85.8 0.6 copy.12
Async XLA Ops:
  0.6 1.6 %copy-start = (bf16[512,2048]{1,0:T(8,128)(2,1)S(1)}, bf16[512,2048]{1,0:T(8,128)(2,1)}, u32[]{:S(2)}) copy-start(bf16[512,2048]{1,0:T(8,128)(2,1)} %tok_hbm.1) | copy-start | bytes 6291460
  2.2 0.9 %copy-start.1 = (f32[64,512]{1,0:T(8,128)S(1)}, f32[64,512]{1,0:T(8,128)}, u32[]{:S(2)}) copy-start(f32[64,512]{1,0:T(8,128)} %upw_ref.1) | copy-start | bytes 393220
  3.1 0.9 %copy-start.2 = (f32[256,128]{1,0:T(8,128)S(1)}, f32[256,128]{1,0:T(8,128)}, u32[]{:S(2)}) copy-start(f32[256,128]{1,0:T(8,128)} %dnw_ref.1) | copy-start | bytes 393220
  4.0 0.7 copy-start.3

commit v2 on v0

v2 whole, which is shorter than its diff:
```python
import jax
import jax.numpy as jnp
from jax import lax
from jax.experimental import pallas as pl
from jax.experimental.pallas import tpu as pltpu
from jax.sharding import PartitionSpec as P

MESH = pl.DeviceIdType.MESH
F32 = jnp.float32
BF16 = jnp.bfloat16

TOK = 512
D = 2048
UNITS = 256
HALF = 128
NT = 4
TC = TOK // NT
H_CHUNKS = ((0, 2, 256), (1, NT, TC))


def numbered(*sizes):
    firsts, at = [], 0
    for size in sizes:
        firsts.append(at)
        at += size
    return (*firsts, at)


UP1, UPX, UPC, DNG, DNX, DNC, DTY, DTX, DTC, HY, RS, N_MSG = numbered(
    8, 12, 16, 1, 6, 8, 4, 3, 4, 6 + 3 * NT, 3 * NT
)


def kernel(
    tok_hbm, gain_hbm, upw_hbm, dnw_hbm,
    up_out, dn_out, mix_ref,
    gain_ref, upw_ref, dnw_ref,
    u_send, up_buf, dn_buf, dt_send, dt_buf, nrm, h_buf,
    s1, r1, k1, s2, r2, k2, s3, r3, k3,
    ssem, rsem, lsem,
):
    g = lax.axis_index("gr")
    f = lax.axis_index("fs")
    t = lax.axis_index("tp")
    zl, y = f // 4, f % 4
    x, k = t // 2, t % 2
    ok = 1 - k
    og = 1 - g

    def dev(gg, zz, yy, xx, kk):
        return (gg, zz * 4 + yy, xx * 2 + kk)

    def message(src, dst, i, to, j=None):
        return pltpu.make_async_remote_copy(
            src_ref=src, dst_ref=dst,
            send_sem=ssem.at[i], recv_sem=rsem.at[i if j is None else j],
            device_id=to, device_id_type=MESH,
        )

    sent = []

    def send(src, dst, i, to, j=None):
        copy = message(src, dst, i, to, j)
        copy.start()
        sent.append(copy)

    to_core = dev(g, zl, y, x, ok)

    def arrived(dst, i):
        message(dst, dst, 0, to_core, i).wait_recv()

    steps = (2, 1, 3)
    x_to = [dev(g, zl, y, (x + s) % 4, k) for s in steps]
    x_from = [(x + 4 - s) % 4 for s in steps]
    y_to = [dev(g, zl, (y + s) % 4, x, k) for s in steps]
    y_from = [(y + 4 - s) % 4 for s in steps]
    b0, b1, b2 = zl % 2, (zl // 2) % 2, zl // 4
    to_z1 = dev(g, zl + 1 - 2 * b0, y, x, k)
    to_z2 = dev(g, zl + 2 - 4 * b1, y, x, k)
    to_z4 = dev(g, zl + 4 - 8 * b2, y, x, k)
    to_gr = dev(og, zl, y, x, k)

    xs, ks, hs = zl % 4, y // 2, y % 2

    def a_of(xx):
        return (xx - xs - hs - 2 * g + 8) % 4

    a_me = a_of(x)
    sources = [
        (q * 2 + w, dev(b2, a_me + 4 * q, 2 * ok + w, xs, ks)) for q in range(2) for w in range(2)
    ]

    barrier = pltpu.get_barrier_semaphore()
    greet = [s for _, s in sources] + [to_gr, *x_to, *y_to, to_z1, to_z2, to_z4, to_core]
    for who in greet:
        pl.semaphore_signal(barrier, inc=1, device_id=who, device_id_type=MESH)

    loads = [
        pltpu.make_async_copy(src, dst, lsem.at[i])
        for i, (src, dst) in enumerate(
            ((gain_hbm, gain_ref), (upw_hbm, upw_ref), (dnw_hbm, dnw_ref), (tok_hbm, nrm))
        )
    ]
    for load in loads:
        load.start()

    loads[0].wait()
    loads[1].wait()
    rows = lax.broadcasted_iota(jnp.int32, (64, 64), 0)
    cols = lax.broadcasted_iota(jnp.int32, (64, 64), 1)
    gain_wide = jnp.broadcast_to(gain_ref[...], (64, 64))
    gain = jnp.sum(jnp.where(rows == cols, gain_wide, 0.0), axis=1, keepdims=True)
    for h in range(2):
        u_send[h] = (gain * upw_ref[:, h * 256 : (h + 1) * 256]).astype(BF16)

    def dn_cols(gg, xx, kk):
        return pl.ds(pl.multiple_of((gg * 8 + xx * 2 + kk) * 128, 128), 128)

    def dn_piece(gg, xx, kk):
        return dn_buf.at[:, dn_cols(gg, xx, kk)]

    loads[2].wait()
    dn_mine = dnw_ref[...]
    dn_buf[:, dn_cols(g, x, k)] = dn_mine.astype(BF16)

    dt_mine = dn_mine.T.astype(BF16)
    for h in range(2):
        dt_send[h, pl.ds(pl.multiple_of(g * 64, 64), 64), :] = dt_mine[h * 64 : (h + 1) * 64]

    pl.semaphore_wait(barrier, len(greet))

    def up_piece(xx, q, kk, u):
        start = ((a_of(xx) + 4 * q) * 4 + 2 * (1 - kk)) * 64
        return up_buf.at[pl.ds(pl.multiple_of(start, 128), 128), pl.ds(u * HALF, HALF)]

    j_me = b2 * 2 + y % 2
    for u in range(2):
        for gg in range(2):
            for h in range(2):
                xx = (x + zl + h + 2 * gg) % 4
                to = (gg, (4 * g + x) * 4 + 2 * k + h, xx * 2 + (1 - y // 2))
                slot = up_buf.at[pl.ds(pl.multiple_of(f * 64, 64), 64), pl.ds(u * HALF, HALF)]
                src = u_send.at[h, :, pl.ds(u * HALF, HALF)]
                send(src, slot, UP1 + u * 4 + gg * 2 + h, to, UP1 + u * 4 + j_me)

    loads[3].wait()

    def norm_rows(i, _):
        at = pl.ds(pl.multiple_of(i * 16, 16), 16)
        wide = nrm[at, :].astype(F32)
        scale = lax.rsqrt(jnp.mean(wide * wide, axis=-1, keepdims=True) + 1e-06)
        nrm[at, :] = (wide * scale).astype(BF16)
        return 0

    lax.fori_loop(0, TOK // 32, norm_rows, 0)
    send(dn_piece(g, x, k), dn_piece(g, x, k), DNG, to_gr)
    lax.fori_loop(TOK // 32, TOK // 16, norm_rows, 0)

    for u in range(2):
        for j, _ in sources:
            q, w = j // 2, j % 2
            start = ((a_me + 4 * q) * 4 + 2 * ok + w) * 64
            slot = up_buf.at[pl.ds(pl.multiple_of(start, 64), 64), pl.ds(u * HALF, HALF)]
            arrived(slot, UP1 + u * 4 + j)
            if w == 1:
                piece = up_piece(x, q, k, u)
                for d in range(3):
                    send(piece, piece, UPX + u * 6 + q * 3 + d, x_to[d])
                send(piece, piece, UPC + u * 8 + q * 4, to_core)

    def up_to_core(u):
        for d in (1, 2, 0):
            for q in range(2):
                piece = up_piece(x_from[d], q, k, u)
                arrived(piece, UPX + u * 6 + q * 3 + d)
                send(piece, piece, UPC + u * 8 + q * 4 + 1 + d, to_core)

    def hidden_half(u):
        for q in range(2):
            arrived(up_piece(x, q, ok, u), UPC + u * 8 + q * 4)
            for d in range(3):
                arrived(up_piece(x_from[d], q, ok, u), UPC + u * 8 + q * 4 + 1 + d)
        _, count, size = H_CHUNKS[u]
        units = pl.ds(u * HALF, HALF)
        for part in range(2):
            at = pl.ds(part * 256, 256)
            pre = jnp.dot(nrm[at, :], up_buf[:, units], preferred_element_type=F32)
            pre = jnp.maximum(pre, 0.0)
            h_buf[y, at, units] = (pre * pre).astype(BF16)
            for j in range(part * count // 2, (part + 1) * count // 2):
                piece = h_buf.at[y, pl.ds(j * size, size), units]
                for d in range(3):
                    send(piece, piece, HY + u * 6 + j * 3 + d, y_to[d])

    up_to_core(0)
    hidden_half(0)

    arrived(dn_piece(og, x, k), DNG)

    def dt_rows(xx):
        return pl.ds(pl.multiple_of(((xx % 2) * 4 + (xx // 2) * 2) * 64, 128), 128)

    dt_other = dn_buf[:, dn_cols(og, x, k)].astype(F32).T.astype(BF16)
    for h in range(2):
        dt_send[h, pl.ds(pl.multiple_of(og * 64, 64), 64), :] = dt_other[h * 64 : (h + 1) * 64]

    def dt_to_y(h):
        return message(
            dt_send.at[h], dt_buf.at[y, dt_rows(x), :], DTY + h, dev(g, zl, 2 * k + h, x, k), DTY + y
        )

    for h in range(2):

        @pl.when(2 * k + h != y)
        def _():
            dt_to_y(h).start()

        @pl.when(2 * k + h == y)
        def _():
            dt_buf[y, dt_rows(x), :] = dt_send[h]

    for q in range(2):
        piece = dn_piece(q, x, k)
        for d in range(3):
            send(piece, piece, DNX + q * 3 + d, x_to[d])
        send(piece, piece, DNC + q * 4, to_core)

    up_to_core(1)
    hidden_half(1)
    up_copy = pltpu.make_async_copy(up_buf, up_out, lsem.at[0])
    up_copy.start()

    owner = ks == k

    def dt_piece(xx):
        return dt_buf.at[:, dt_rows(xx), :]

    def dt_along_x():
        return [message(dt_piece(x), dt_piece(x), DTX + d, x_to[d]) for d in range(3)] + [
            message(dt_piece(x), dt_piece(x), DTC, to_core)
        ]

    def dt_to_core(d):
        return message(dt_piece(x_from[d]), dt_piece(x_from[d]), DTC + 1 + d, to_core)

    @pl.when(owner)
    def _():
        for src in range(4):

            @pl.when(y != src)
            def _():
                arrived(dt_buf.at[src, dt_rows(x), :], DTY + src)

        for copy in dt_along_x():
            copy.start()

    for q in range(2):
        for d in (1, 2, 0):
            piece = dn_piece(q, x_from[d], k)
            arrived(piece, DNX + q * 3 + d)
            send(piece, piece, DNC + q * 4 + 1 + d, to_core)

    @pl.when(owner)
    def _():
        for d in (1, 2, 0):
            arrived(dt_piece(x_from[d]), DTX + d)
            dt_to_core(d).start()

    @pl.when(jnp.logical_not(owner))
    def _():
        arrived(dt_piece(x), DTC)
        for d in range(3):
            arrived(dt_piece(x_from[d]), DTC + 1 + d)

    def times_hidden(rows_at, size, at):
        total = jnp.zeros((size, TC), F32)
        for yy in range(4):
            total += lax.dot_general(
                dt_buf[yy, rows_at, :], h_buf[yy, at, :],
                (((1,), (1,)), ((), ())), preferred_element_type=F32,
            )
        return total

    def aligned(start, size):
        return pl.ds(pl.multiple_of(start, 64), size)

    def hidden_in(u, j):
        _, _, size = H_CHUNKS[u]
        for d in range(3):
            arrived(h_buf.at[y_from[d], pl.ds(j * size, size), pl.ds(u * HALF, HALF)], HY + u * 6 + j * 3 + d)

    for j in range(NT):
        at = pl.ds(j * TC, TC)
        if j % (NT // 2) == 0:
            hidden_in(0, j // (NT // 2))
        hidden_in(1, j)
        s1[j] = times_hidden(aligned((1 - b0) * 256, 256), 256, at).astype(BF16)
        send(s1.at[j], r1.at[j], RS + 3 * j, to_z1)
        k1[j] = times_hidden(aligned(b0 * 256, 256), 256, at)

    for j in range(NT):
        arrived(r1.at[j], RS + 3 * j)
        out, keep = aligned((1 - b1) * 128, 128), aligned(b1 * 128, 128)
        s2[j] = (k1[j, out, :] + r1[j, out, :].astype(F32)).astype(BF16)
        send(s2.at[j], r2.at[j], RS + 3 * j + 1, to_z2)
        k2[j] = k1[j, keep, :] + r1[j, keep, :].astype(F32)
    for j in range(NT):
        arrived(r2.at[j], RS + 3 * j + 1)
        out, keep = aligned((1 - b2) * 64, 64), aligned(b2 * 64, 64)
        s3[j] = (k2[j, out, :] + r2[j, out, :].astype(F32)).astype(BF16)
        send(s3.at[j], r3.at[j], RS + 3 * j + 2, to_z4)
        k3[j] = k2[j, keep, :] + r2[j, keep, :].astype(F32)

    for q in range(2):
        arrived(dn_piece(q, x, ok), DNC + q * 4)
        for d in range(3):
            arrived(dn_piece(q, x_from[d], ok), DNC + q * 4 + 1 + d)
    dn_copy = pltpu.make_async_copy(dn_buf, dn_out, lsem.at[1])
    dn_copy.start()

    for j in range(NT):
        arrived(r3.at[j], RS + 3 * j + 2)
        mix_ref[:, j * TC : (j + 1) * TC] = (k3[j] + r3[j].astype(F32)).astype(BF16)

    for copy in sent:
        copy.wait_send()
    for h in range(2):

        @pl.when(2 * k + h != y)
        def _():
            dt_to_y(h).wait_send()

    @pl.when(owner)
    def _():
        for copy in dt_along_x():
            copy.wait_send()
        for d in range(3):
            dt_to_core(d).wait_send()

    up_copy.wait()
    dn_copy.wait()


def per_device(tokens, norm_gain, up_weight, down_weight):
    hbm = pl.BlockSpec(memory_space=pltpu.HBM)
    vmem = pl.BlockSpec(memory_space=pltpu.VMEM)
    up_block, down_block, mixed = pl.pallas_call(
        kernel,
        out_shape=(
            jax.ShapeDtypeStruct((D, UNITS), BF16),
            jax.ShapeDtypeStruct((UNITS, D), BF16),
            jax.ShapeDtypeStruct((64, TOK), BF16),
        ),
        in_specs=[hbm] * 4,
        out_specs=(hbm, hbm, vmem),
        scratch_shapes=[
            pltpu.VMEM((1, 64), F32),
            pltpu.VMEM((64, 512), F32),
            pltpu.VMEM((256, 128), F32),
            pltpu.VMEM((2, 64, 256), BF16),
            pltpu.VMEM((D, UNITS), BF16),
            pltpu.VMEM((UNITS, D), BF16),
            pltpu.VMEM((2, 128, 256), BF16),
            pltpu.VMEM((4, 512, 256), BF16),
            pltpu.VMEM((TOK, D), BF16),
            pltpu.VMEM((4, TOK, UNITS), BF16),
            pltpu.VMEM((NT, 256, TC), BF16),
            pltpu.VMEM((NT, 256, TC), BF16),
            pltpu.VMEM((NT, 256, TC), F32),
            pltpu.VMEM((NT, 128, TC), BF16),
            pltpu.VMEM((NT, 128, TC), BF16),
            pltpu.VMEM((NT, 128, TC), F32),
            pltpu.VMEM((NT, 64, TC), BF16),
            pltpu.VMEM((NT, 64, TC), BF16),
            pltpu.VMEM((NT, 64, TC), F32),
            pltpu.SemaphoreType.DMA((N_MSG,)),
            pltpu.SemaphoreType.DMA((N_MSG,)),
            pltpu.SemaphoreType.DMA((4,)),
        ],
        compiler_params=pltpu.CompilerParams(
            collective_id=0, has_side_effects=True, vmem_limit_bytes=60 * 1024 * 1024
        ),
        name="handoff",
    )(tokens, norm_gain.reshape(1, 64), up_weight, down_weight)
    return up_block, down_block, mixed.T


def solution(mesh):
    in_specs = (P(("gr", "tp"), None), P("fs"), P("fs", ("gr", "tp")), P("fs", ("gr", "tp")))
    out_specs = (P(None, "fs"), P("fs", None), P(("gr", "tp"), "fs"))
    return jax.shard_map(
        per_device, mesh=mesh, in_specs=in_specs, out_specs=out_specs, check_vma=False
    )
```

time: 287 us -> 87.1 us (0.30)
  waiting for transfers between devices: 239 us -> 0 us
  Pallas kernels: 0 us -> 82.3 us
  between operations: 14.1 us -> 0.66 us
  starting transfers between devices: 12.8 us -> 0 us
  other arithmetic: 5.57 us -> 0 us
  local copies, waits for them, and re-layouts: 9.32 us -> 3.96 us
  matrix products: 5.31 us -> 0 us
    all_to_all x2 -> x0, waiting for transfers between devices: 140 us -> none  [the longest x1 92.4 us: sent_and_summed(): lax.all_to_all(parts, axis, split_axis=0, concat_axis=0, tiled=True)]
    all_gather x1 -> x0, waiting for transfers between devices: 99.7 us -> none  [one_gather(): lines, at, done = (lax.all_gather(vector, axis), 0, [])]
    pallas_call x0 -> x1, Pallas kernels: none -> 82.3 us  [per_device(): pl.pallas_call(kernel, out_shape=(jax.ShapeDtypeStruct((D, UNITS), BF16),...]
    all_to_all x2 -> x0, starting transfers between devices: 12.7 us -> none  [the longest x1 7.76 us: sent_and_summed(): lax.all_to_all(parts, axis, split_axis=0, concat_axis=0, tiled=True)]
    dot_general x1 -> x0, matrix products: 5.31 us -> none  [per_device(): lax.dot_general(down_columns, hidden, (((0,), (1,)), ((), ())), preferred...]
    reduce_sum x2 -> x0, other arithmetic: 3 us -> none  [the longest x1 2.08 us: per_device(): jnp.mean(widened * widened, axis=-1, keepdims=True) + 1e-06]
  transfers between devices with their start and end apart: 3 -> 0, of which waited for: 3 -> 0; matrix products, arithmetic and copies ran while one was open for 2% -> 0% of each run, Pallas kernels for 0% -> 0%
where the time goes in v2:
time: 87.1 us; the launch traced here: 86.9 us
  Pallas kernels  82.3 us (94%)
  local copies, waits for them, and re-layouts  3.96 us (5%)
    pallas_call x1, Pallas kernels, per_device(): pl.pallas_call(kernel, out_shape=(jax.ShapeDtypeStruct((D, UNITS), BF16),...  82.3 us
    unnamed x7, local copies, waits for them, and re-layouts  3.96 us

profile of v2, /device:TPU:1, one launch (start us, length us, event | category | flops | bytes accessed | tf_op | source)
XLA Modules:
  0.0 86.9 jit_solution(2150718546617772219)
XLA Ops:
  0.6 82.3 %handoff.1 = (bf16[2048,256]{1,0:T(8,128)(2,1)}, bf16[256,2048]{1,0:T(8,128)(2,1)}, bf16[64,512]{1,0:T(8,128)(2,1)}) custom-call(bf16[512,2048]{1,0:T(8,128)(2,1)} %tok_hbm.1, f32[1,64]{1,0:T(1,128)} %bitcast.3, f32[64,512]{1,0:T(8,128)} %upw_hbm.1, f32[256,128]{1,0:T(8,128)} %dnw_hbm.1), custom_call_target="tpu_custom_call" | custom-call | tf_op jit(solution)/shard_map/handoff/pallas_call | solution.py:347
  83.0 0.0 copy-start
  83.0 0.0 copy-start.1
  83.0 2.4 %copy.10 = bf16[2048,256]{1,0:T(8,128)(2,1)} copy(bf16[2048,256]{1,0:T(8,128)(2,1)} %get-tuple-element.12) | data formatting | bytes 2097152
  85.3 0.0 copy-done
  85.3 1.0 %copy.11 = bf16[256,2048]{1,0:T(8,128)(2,1)} copy(bf16[256,2048]{1,0:T(8,128)(2,1)S(1)} %copy-done) | data formatting | bytes 2097152
  86.3 0.0 copy-done.1
  86.3 0.6 copy.12
Async XLA Ops:
  83.0 2.4 %copy-start = (bf16[256,2048]{1,0:T(8,128)(2,1)S(1)}, bf16[256,2048]{1,0:T(8,128)(2,1)}, u32[]{:S(2)}) copy-start(bf16[256,2048]{1,0:T(8,128)(2,1)} %get-tuple-element.13) | copy-start | bytes 3145732
  83.0 3.3 %copy-start.1 = (bf16[64,512]{1,0:T(8,128)(2,1)S(1)}, bf16[64,512]{1,0:T(8,128)(2,1)}, u32[]{:S(2)}) copy-start(bf16[64,512]{1,0:T(8,128)(2,1)} %get-tuple-element.8) | copy-start | bytes 196612

commit v3 on v2

--- a/solution.py
+++ b/solution.py
@@ -15,6 +15,7 @@
 HALF = 128
 NT = 4
 TC = TOK // NT
+NORM_A, NORM_B = 20, 32
 H_CHUNKS = ((0, 2, 256), (1, NT, TC))
 
 
@@ -27,15 +28,15 @@
 
 
 UP1, UPX, UPC, DNG, DNX, DNC, DTY, DTX, DTC, HY, RS, N_MSG = numbered(
-    8, 12, 16, 1, 6, 8, 4, 3, 4, 6 + 3 * NT, 3 * NT
+    8, 12, 16, 1, 6, 8, 8, 6, 8, 6 + 3 * NT, 3 * NT
 )
 
 
 def kernel(
     tok_hbm, gain_hbm, upw_hbm, dnw_hbm,
-    up_out, dn_out, mix_ref,
+    up_buf, dn_buf, mix_ref,
     gain_ref, upw_ref, dnw_ref,
-    u_send, up_buf, dn_buf, dt_send, dt_buf, nrm, h_buf,
+    u_send, dt_send, dt_buf, nrm, h_buf,
     s1, r1, k1, s2, r2, k2, s3, r3, k3,
     ssem, rsem, lsem,
 ):
@@ -125,7 +126,7 @@
 
     dt_mine = dn_mine.T.astype(BF16)
     for h in range(2):
-        dt_send[h, pl.ds(pl.multiple_of(g * 64, 64), 64), :] = dt_mine[h * 64 : (h + 1) * 64]
+        dt_send[0, h] = dt_mine[h * 64 : (h + 1) * 64]
 
     pl.semaphore_wait(barrier, len(greet))
 
@@ -143,6 +144,76 @@
                 src = u_send.at[h, :, pl.ds(u * HALF, HALF)]
                 send(src, slot, UP1 + u * 4 + gg * 2 + h, to, UP1 + u * 4 + j_me)
 
+    owner = ks == k
+    halves = (g, og)
+
+    def dt_rows(part, xx):
+        return pl.ds(pl.multiple_of(((xx % 2) * 4 + (xx // 2) * 2 + halves[part]) * 64, 64), 64)
+
+    def dt_piece(part, xx):
+        return dt_buf.at[:, dt_rows(part, xx), :]
+
+    def dt_to_y(part, h):
+        return message(
+            dt_send.at[part, h], dt_buf.at[y, dt_rows(part, x), :],
+            DTY + part * 4 + h, dev(g, zl, 2 * k + h, x, k), DTY + part * 4 + y,
+        )
+
+    def dt_over_y(part):
+        for h in range(2):
+
+            @pl.when(2 * k + h != y)
+            def _():
+                dt_to_y(part, h).start()
+
+            @pl.when(2 * k + h == y)
+            def _():
+                dt_buf[y, dt_rows(part, x), :] = dt_send[part, h]
+
+    def dt_from_x(part):
+        piece = dt_piece(part, x)
+        return [message(piece, piece, DTX + part * 3 + d, x_to[d]) for d in range(3)] + [
+            message(piece, piece, DTC + part * 4, to_core)
+        ]
+
+    def dt_over_x(part):
+        @pl.when(owner)
+        def _():
+            for src in range(4):
+
+                @pl.when(y != src)
+                def _():
+                    arrived(dt_buf.at[src, dt_rows(part, x), :], DTY + part * 4 + src)
+
+            for copy in dt_from_x(part):
+                copy.start()
+
+    def dt_to_core(part, d):
+        piece = dt_piece(part, x_from[d])
+        return message(piece, piece, DTC + part * 4 + 1 + d, to_core)
+
+    def dt_over_core(part):
+        @pl.when(owner)
+        def _():
+            for d in (1, 2, 0):
+                arrived(dt_piece(part, x_from[d]), DTX + part * 3 + d)
+                dt_to_core(part, d).start()
+
+    def dn_over_x(part):
+        piece = dn_piece(halves[part], x, k)
+        for d in range(3):
+            send(piece, piece, DNX + part * 3 + d, x_to[d])
+        send(piece, piece, DNC + part * 4, to_core)
+
+    def dn_over_core(part):
+        for d in (1, 2, 0):
+            piece = dn_piece(halves[part], x_from[d], k)
+            arrived(piece, DNX + part * 3 + d)
+            send(piece, piece, DNC + part * 4 + 1 + d, to_core)
+
+    dt_over_y(0)
+    dn_over_x(0)
+
     loads[3].wait()
 
     def norm_rows(i, _):
@@ -152,9 +223,11 @@
         nrm[at, :] = (wide * scale).astype(BF16)
         return 0
 
-    lax.fori_loop(0, TOK // 32, norm_rows, 0)
+    lax.fori_loop(0, NORM_A, norm_rows, 0)
+    dt_over_x(0)
+    lax.fori_loop(NORM_A, NORM_B, norm_rows, 0)
     send(dn_piece(g, x, k), dn_piece(g, x, k), DNG, to_gr)
-    lax.fori_loop(TOK // 32, TOK // 16, norm_rows, 0)
+    lax.fori_loop(NORM_B, TOK // 16, norm_rows, 0)
 
     for u in range(2):
         for j, _ in sources:
@@ -192,85 +265,30 @@
                 for d in range(3):
                     send(piece, piece, HY + u * 6 + j * 3 + d, y_to[d])
 
+    dt_over_core(0)
     up_to_core(0)
-    hidden_half(0)
-
     arrived(dn_piece(og, x, k), DNG)
-
-    def dt_rows(xx):
-        return pl.ds(pl.multiple_of(((xx % 2) * 4 + (xx // 2) * 2) * 64, 128), 128)
-
     dt_other = dn_buf[:, dn_cols(og, x, k)].astype(F32).T.astype(BF16)
     for h in range(2):
-        dt_send[h, pl.ds(pl.multiple_of(og * 64, 64), 64), :] = dt_other[h * 64 : (h + 1) * 64]
-
-    def dt_to_y(h):
-        return message(
-            dt_send.at[h], dt_buf.at[y, dt_rows(x), :], DTY + h, dev(g, zl, 2 * k + h, x, k), DTY + y
-        )
-
-    for h in range(2):
-
-        @pl.when(2 * k + h != y)
-        def _():
-            dt_to_y(h).start()
-
-        @pl.when(2 * k + h == y)
-        def _():
-            dt_buf[y, dt_rows(x), :] = dt_send[h]
-
-    for q in range(2):
-        piece = dn_piece(q, x, k)
-        for d in range(3):
-            send(piece, piece, DNX + q * 3 + d, x_to[d])
-        send(piece, piece, DNC + q * 4, to_core)
-
+        dt_send[1, h] = dt_other[h * 64 : (h + 1) * 64]
+    dt_over_y(1)
+
+    hidden_half(0)
+
+    dt_over_x(1)
     up_to_core(1)
     hidden_half(1)
-    up_copy = pltpu.make_async_copy(up_buf, up_out, lsem.at[0])
-    up_copy.start()
-
-    owner = ks == k
-
-    def dt_piece(xx):
-        return dt_buf.at[:, dt_rows(xx), :]
-
-    def dt_along_x():
-        return [message(dt_piece(x), dt_piece(x), DTX + d, x_to[d]) for d in range(3)] + [
-            message(dt_piece(x), dt_piece(x), DTC, to_core)
-        ]
-
-    def dt_to_core(d):
-        return message(dt_piece(x_from[d]), dt_piece(x_from[d]), DTC + 1 + d, to_core)
-
-    @pl.when(owner)
-    def _():
-        for src in range(4):
-
-            @pl.when(y != src)
-            def _():
-                arrived(dt_buf.at[src, dt_rows(x), :], DTY + src)
-
-        for copy in dt_along_x():
-            copy.start()
-
-    for q in range(2):
-        for d in (1, 2, 0):
-            piece = dn_piece(q, x_from[d], k)
-            arrived(piece, DNX + q * 3 + d)
-            send(piece, piece, DNC + q * 4 + 1 + d, to_core)
-
-    @pl.when(owner)
-    def _():
-        for d in (1, 2, 0):
-            arrived(dt_piece(x_from[d]), DTX + d)
-            dt_to_core(d).start()
+
+    dn_over_x(1)
+
+    dt_over_core(1)
 
     @pl.when(jnp.logical_not(owner))
     def _():
-        arrived(dt_piece(x), DTC)
-        for d in range(3):
-            arrived(dt_piece(x_from[d]), DTC + 1 + d)
+        for part in range(2):
+            arrived(dt_piece(part, x), DTC + part * 4)
+            for d in range(3):
+                arrived(dt_piece(part, x_from[d]), DTC + part * 4 + 1 + d)
 
     def times_hidden(rows_at, size, at):
         total = jnp.zeros((size, TC), F32)
@@ -311,12 +329,13 @@
         send(s3.at[j], r3.at[j], RS + 3 * j + 2, to_z4)
         k3[j] = k2[j, keep, :] + r2[j, keep, :].astype(F32)
 
-    for q in range(2):
-        arrived(dn_piece(q, x, ok), DNC + q * 4)
+    dn_over_core(0)
+    dn_over_core(1)
+
+    for part in range(2):
+        arrived(dn_piece(halves[part], x, ok), DNC + part * 4)
         for d in range(3):
-            arrived(dn_piece(q, x_from[d], ok), DNC + q * 4 + 1 + d)
-    dn_copy = pltpu.make_async_copy(dn_buf, dn_out, lsem.at[1])
-    dn_copy.start()
+            arrived(dn_piece(halves[part], x_from[d], ok), DNC + part * 4 + 1 + d)
 
     for j in range(NT):
         arrived(r3.at[j], RS + 3 * j + 2)
@@ -324,21 +343,30 @@
 
     for copy in sent:
         copy.wait_send()
-    for h in range(2):
-
-        @pl.when(2 * k + h != y)
+    for part in range(2):
+        for h in range(2):
+
+            @pl.when(2 * k + h != y)
+            def _():
+                dt_to_y(part, h).wait_send()
+
+        @pl.when(owner)
         def _():
-            dt_to_y(h).wait_send()
-
-    @pl.when(owner)
-    def _():
-        for copy in dt_along_x():
-            copy.wait_send()
-        for d in range(3):
-            dt_to_core(d).wait_send()
-
-    up_copy.wait()
-    dn_copy.wait()
+            for copy in dt_from_x(part):
+                copy.wait_send()
+            for d in range(3):
+                dt_to_core(part, d).wait_send()
+
+
+def write_out(up_ref, dn_ref, mix_ref, up_hbm, dn_hbm, mix_hbm, lsem):
+    copies = [
+        pltpu.make_async_copy(src, dst, lsem.at[i])
+        for i, (src, dst) in enumerate(((up_ref, up_hbm), (dn_ref, dn_hbm), (mix_ref, mix_hbm)))
+    ]
+    for copy in copies:
+        copy.start()
+    for copy in copies:
+        copy.wait()
 
 
 def per_device(tokens, norm_gain, up_weight, down_weight):
@@ -352,15 +380,13 @@
             jax.ShapeDtypeStruct((64, TOK), BF16),
         ),
         in_specs=[hbm] * 4,
-        out_specs=(hbm, hbm, vmem),
+        out_specs=(vmem,) * 3,
         scratch_shapes=[
             pltpu.VMEM((1, 64), F32),
             pltpu.VMEM((64, 512), F32),
             pltpu.VMEM((256, 128), F32),
             pltpu.VMEM((2, 64, 256), BF16),
-            pltpu.VMEM((D, UNITS), BF16),
-            pltpu.VMEM((UNITS, D), BF16),
-            pltpu.VMEM((2, 128, 256), BF16),
+            pltpu.VMEM((2, 2, 64, 256), BF16),
             pltpu.VMEM((4, 512, 256), BF16),
             pltpu.VMEM((TOK, D), BF16),
             pltpu.VMEM((4, TOK, UNITS), BF16),
@@ -378,10 +404,23 @@
             pltpu.SemaphoreType.DMA((4,)),
         ],
         compiler_params=pltpu.CompilerParams(
-            collective_id=0, has_side_effects=True, vmem_limit_bytes=60 * 1024 * 1024
+            collective_id=0, has_side_effects=True, vmem_limit_bytes=16 * 1024 * 1024
         ),
         name="handoff",
-    )(tokens, norm_gain.reshape(1, 64), up_weight, down_weight)
+    )(*(
+        pltpu.with_memory_space_constraint(a, pltpu.HBM)
+        for a in (tokens, norm_gain.reshape(1, 64), up_weight, down_weight)
+    ))
+    results = (up_block, down_block, mixed)
+    up_block, down_block, mixed = pl.pallas_call(
+        write_out,
+        out_shape=tuple(jax.ShapeDtypeStruct(a.shape, a.dtype) for a in results),
+        in_specs=[vmem] * 3,
+        out_specs=(hbm,) * 3,
+        scratch_shapes=[pltpu.SemaphoreType.DMA((3,))],
+        compiler_params=pltpu.CompilerParams(vmem_limit_bytes=8 * 1024 * 1024),
+        name="write_out",
+    )(*results)
     return up_block, down_block, mixed.T
 
 

time: 87.1 us -> 77.1 us (0.89)
  Pallas kernels: 82.3 us -> 76.3 us
  local copies, waits for them, and re-layouts: 3.96 us -> 0 us
    pallas_call x1, Pallas kernels: 82.3 us -> 75 us  [per_device(): pl.pallas_call(kernel, out_shape=(jax.ShapeDtypeStruct((D, UNITS), BF16),...]
    unnamed x7 -> x0, local copies, waits for them, and re-layouts: 3.96 us -> none
    pallas_call x0 -> x1, Pallas kernels: none -> 1.35 us  [per_device(): pl.pallas_call(write_out, out_shape=tuple((jax.ShapeDtypeStruct(a.shape,...]
where the time goes in v3:
time: 77.1 us; the launch traced here: 76.9 us
  Pallas kernels  76.3 us (99%)
    pallas_call x1, Pallas kernels, per_device(): pl.pallas_call(kernel, out_shape=(jax.ShapeDtypeStruct((D, UNITS), BF16),...  75 us

profile of v3, /device:TPU:1, one launch (start us, length us, event | category | flops | bytes accessed | tf_op | source)
XLA Modules:
  0.0 76.9 jit_solution(10944434807348095217)
XLA Ops:
  0.6 75.0 %handoff.1 = (bf16[2048,256]{1,0:T(8,128)(2,1)S(1)}, bf16[256,2048]{1,0:T(8,128)(2,1)S(1)}, bf16[64,512]{1,0:T(8,128)(2,1)S(1)}) custom-call(bf16[512,2048]{1,0:T(8,128)(2,1)} %tok_hbm.1, f32[1,64]{1,0:T(1,128)} %bitcast.2, f32[64,512]{1,0:T(8,128)} %upw_hbm.1, f32[256,128]{1,0:T(8,128)} %dnw_hbm.1), custom_call_target="tpu_custom_call" | custom-call | tf_op jit(solution)/shard_map/handoff/pallas_call | solution.py:375
  75.6 1.3 %write_out.1 = (bf16[2048,256]{1,0:T(8,128)(2,1)}, bf16[256,2048]{1,0:T(8,128)(2,1)}, bf16[64,512]{1,0:T(8,128)(2,1)}) custom-call(bf16[2048,256]{1,0:T(8,128)(2,1)S(1)} %get-tuple-element.9.up_ref, bf16[256,2048]{1,0:T(8,128)(2,1)S(1)} %get-tuple-element.10.dn_ref, bf16[64,512]{1,0:T(8,128)(2,1)S(1)} %get-tuple-element.11.mix_ref), custom_call_target="tpu_custom_call" | custom-call | tf_op jit(solution)/shard_map/write_out/pallas_call | solution.py:415

commit v4 on v3

--- a/solution.py
+++ b/solution.py
@@ -15,8 +15,8 @@
 HALF = 128
 NT = 4
 TC = TOK // NT
-NORM_A, NORM_B = 20, 32
-H_CHUNKS = ((0, 2, 256), (1, NT, TC))
+NORM_U, NORM_A, NORM_B = 18, 24, 32
+WIDE = 256
 
 
 def numbered(*sizes):
@@ -27,8 +27,8 @@
     return (*firsts, at)
 
 
-UP1, UPX, UPC, DNG, DNX, DNC, DTY, DTX, DTC, HY, RS, N_MSG = numbered(
-    8, 12, 16, 1, 6, 8, 8, 6, 8, 6 + 3 * NT, 3 * NT
+UP1, UPF, UPX, UPC, DNG, DNX, DNC, DTY, DTX, DTC, HY, RS, N_MSG = numbered(
+    8, 4, 12, 16, 1, 6, 8, 8, 6, 8, 12, 3 * NT
 )
 
 
@@ -38,7 +38,7 @@
     gain_ref, upw_ref, dnw_ref,
     u_send, dt_send, dt_buf, nrm, h_buf,
     s1, r1, k1, s2, r2, k2, s3, r3, k3,
-    ssem, rsem, lsem,
+    ssem, rsem, lsem, far_sem,
 ):
     g = lax.axis_index("gr")
     f = lax.axis_index("fs")
@@ -82,9 +82,11 @@
     to_gr = dev(og, zl, y, x, k)
 
     xs, ks, hs = zl % 4, y // 2, y % 2
+    relayed = jnp.logical_and(g == 1, b2 == 0)
+    relays = jnp.logical_and(g == 0, b2 == 0)
 
     def a_of(xx):
-        return (xx - xs - hs - 2 * g + 8) % 4
+        return (xx - xs - hs - 2 * g * b2 + 8) % 4
 
     a_me = a_of(x)
     sources = [
@@ -92,9 +94,21 @@
     ]
 
     barrier = pltpu.get_barrier_semaphore()
-    greet = [s for _, s in sources] + [to_gr, *x_to, *y_to, to_z1, to_z2, to_z4, to_core]
-    for who in greet:
+
+    def greet(who):
         pl.semaphore_signal(barrier, inc=1, device_id=who, device_id_type=MESH)
+
+    @pl.when(jnp.logical_not(relayed))
+    def _():
+        for _, source in sources:
+            greet(source)
+
+    @pl.when(g == 0)
+    def _():
+        greet(to_gr)
+
+    for who in (*x_to, *y_to, to_z1, to_z2, to_z4, to_core):
+        greet(who)
 
     loads = [
         pltpu.make_async_copy(src, dst, lsem.at[i])
@@ -128,21 +142,43 @@
     for h in range(2):
         dt_send[0, h] = dt_mine[h * 64 : (h + 1) * 64]
 
-    pl.semaphore_wait(barrier, len(greet))
+    @pl.when(g == 0)
+    def _():
+        pl.semaphore_wait(barrier, 12)
+
+    @pl.when(g == 1)
+    def _():
+        pl.semaphore_wait(barrier, 15)
+        pl.semaphore_signal(far_sem, inc=1, device_id=to_gr, device_id_type=MESH)
+
 
     def up_piece(xx, q, kk, u):
         start = ((a_of(xx) + 4 * q) * 4 + 2 * (1 - kk)) * 64
         return up_buf.at[pl.ds(pl.multiple_of(start, 128), 128), pl.ds(u * HALF, HALF)]
 
     j_me = b2 * 2 + y % 2
-    for u in range(2):
-        for gg in range(2):
+
+    def up_message(u, gg, h):
+        xx = (x + zl + h + 2 * gg) % 4
+        to = (gg, (4 * g + x) * 4 + 2 * k + h, xx * 2 + (1 - y // 2))
+        slot = up_buf.at[pl.ds(pl.multiple_of(f * 64, 64), 64), pl.ds(u * HALF, HALF)]
+        src = u_send.at[h, :, pl.ds(u * HALF, HALF)]
+        return message(src, slot, UP1 + u * 4 + gg * 2 + h, to, UP1 + u * 4 + j_me)
+
+    def up_first(u):
+        for h in range(2):
+            up_message(u, 0, h).start()
+
+        @pl.when(g == 1)
+        def _():
             for h in range(2):
-                xx = (x + zl + h + 2 * gg) % 4
-                to = (gg, (4 * g + x) * 4 + 2 * k + h, xx * 2 + (1 - y // 2))
-                slot = up_buf.at[pl.ds(pl.multiple_of(f * 64, 64), 64), pl.ds(u * HALF, HALF)]
-                src = u_send.at[h, :, pl.ds(u * HALF, HALF)]
-                send(src, slot, UP1 + u * 4 + gg * 2 + h, to, UP1 + u * 4 + j_me)
+                up_message(u, 1, h).start()
+
+    def up_relay(u, q):
+        piece = up_piece(x, q, k, u)
+        return message(piece, piece, UPF + u * 2 + q, to_gr)
+
+    up_first(0)
 
     owner = ks == k
     halves = (g, og)
@@ -223,23 +259,43 @@
         nrm[at, :] = (wide * scale).astype(BF16)
         return 0
 
-    lax.fori_loop(0, NORM_A, norm_rows, 0)
+    lax.fori_loop(0, NORM_U, norm_rows, 0)
+    up_first(1)
+    lax.fori_loop(NORM_U, NORM_A, norm_rows, 0)
     dt_over_x(0)
     lax.fori_loop(NORM_A, NORM_B, norm_rows, 0)
+    lax.fori_loop(NORM_B, TOK // 16, norm_rows, 0)
+
+    @pl.when(g == 0)
+    def _():
+        pl.semaphore_wait(far_sem, 1)
+
+    def up_in(u):
+        for q in range(2):
+
+            @pl.when(relayed)
+            def _():
+                arrived(up_piece(x, q, k, u), UPF + u * 2 + q)
+
+            @pl.when(jnp.logical_not(relayed))
+            def _():
+                for w in range(2):
+                    start = ((a_me + 4 * q) * 4 + 2 * ok + w) * 64
+                    slot = up_buf.at[pl.ds(pl.multiple_of(start, 64), 64), pl.ds(u * HALF, HALF)]
+                    arrived(slot, UP1 + u * 4 + q * 2 + w)
+
+            @pl.when(relays)
+            def _():
+                up_relay(u, q).start()
+
+            piece = up_piece(x, q, k, u)
+            for d in range(3):
+                send(piece, piece, UPX + u * 6 + q * 3 + d, x_to[d])
+            send(piece, piece, UPC + u * 8 + q * 4, to_core)
+
     send(dn_piece(g, x, k), dn_piece(g, x, k), DNG, to_gr)
-    lax.fori_loop(NORM_B, TOK // 16, norm_rows, 0)
-
-    for u in range(2):
-        for j, _ in sources:
-            q, w = j // 2, j % 2
-            start = ((a_me + 4 * q) * 4 + 2 * ok + w) * 64
-            slot = up_buf.at[pl.ds(pl.multiple_of(start, 64), 64), pl.ds(u * HALF, HALF)]
-            arrived(slot, UP1 + u * 4 + j)
-            if w == 1:
-                piece = up_piece(x, q, k, u)
-                for d in range(3):
-                    send(piece, piece, UPX + u * 6 + q * 3 + d, x_to[d])
-                send(piece, piece, UPC + u * 8 + q * 4, to_core)
+    up_in(0)
+    up_in(1)
 
     def up_to_core(u):
         for d in (1, 2, 0):
@@ -248,22 +304,26 @@
                 arrived(piece, UPX + u * 6 + q * 3 + d)
                 send(piece, piece, UPC + u * 8 + q * 4 + 1 + d, to_core)
 
+    def hidden_out(u, part):
+        piece = h_buf.at[y, pl.ds(part * WIDE, WIDE), pl.ds(u * HALF, HALF)]
+        for d in range(3):
+            send(piece, piece, HY + u * 6 + part * 3 + d, y_to[d])
+
     def hidden_half(u):
         for q in range(2):
             arrived(up_piece(x, q, ok, u), UPC + u * 8 + q * 4)
             for d in range(3):
                 arrived(up_piece(x_from[d], q, ok, u), UPC + u * 8 + q * 4 + 1 + d)
-        _, count, size = H_CHUNKS[u]
         units = pl.ds(u * HALF, HALF)
         for part in range(2):
-            at = pl.ds(part * 256, 256)
+            at = pl.ds(part * WIDE, WIDE)
             pre = jnp.dot(nrm[at, :], up_buf[:, units], preferred_element_type=F32)
             pre = jnp.maximum(pre, 0.0)
             h_buf[y, at, units] = (pre * pre).astype(BF16)
-            for j in range(part * count // 2, (part + 1) * count // 2):
-                piece = h_buf.at[y, pl.ds(j * size, size), units]
-                for d in range(3):
-                    send(piece, piece, HY + u * 6 + j * 3 + d, y_to[d])
+            if (u, part) != (0, 1):
+                hidden_out(u, part)
+            if (u, part) == (1, 0):
+                hidden_out(0, 1)
 
     dt_over_core(0)
     up_to_core(0)
@@ -290,8 +350,9 @@
             for d in range(3):
                 arrived(dt_piece(part, x_from[d]), DTC + part * 4 + 1 + d)
 
-    def times_hidden(rows_at, size, at):
-        total = jnp.zeros((size, TC), F32)
+    def times_hidden(first, at):
+        rows_at = pl.ds(pl.multiple_of(first, 256), 256)
+        total = jnp.zeros((256, WIDE), F32)
         for yy in range(4):
             total += lax.dot_general(
                 dt_buf[yy, rows_at, :], h_buf[yy, at, :],
@@ -302,19 +363,21 @@
     def aligned(start, size):
         return pl.ds(pl.multiple_of(start, 64), size)
 
-    def hidden_in(u, j):
-        _, _, size = H_CHUNKS[u]
-        for d in range(3):
-            arrived(h_buf.at[y_from[d], pl.ds(j * size, size), pl.ds(u * HALF, HALF)], HY + u * 6 + j * 3 + d)
-
-    for j in range(NT):
-        at = pl.ds(j * TC, TC)
-        if j % (NT // 2) == 0:
-            hidden_in(0, j // (NT // 2))
-        hidden_in(1, j)
-        s1[j] = times_hidden(aligned((1 - b0) * 256, 256), 256, at).astype(BF16)
-        send(s1.at[j], r1.at[j], RS + 3 * j, to_z1)
-        k1[j] = times_hidden(aligned(b0 * 256, 256), 256, at)
+    for part in range(2):
+        at = pl.ds(part * WIDE, WIDE)
+        for u in range(2):
+            for d in range(3):
+                piece = h_buf.at[y_from[d], at, pl.ds(u * HALF, HALF)]
+                arrived(piece, HY + u * 6 + part * 3 + d)
+        total = times_hidden((1 - b0) * 256, at).astype(BF16)
+        for i in range(WIDE // TC):
+            j = part * (WIDE // TC) + i
+            s1[j] = total[:, i * TC : (i + 1) * TC]
+            send(s1.at[j], r1.at[j], RS + 3 * j, to_z1)
+    for part in range(2):
+        total = times_hidden(b0 * 256, pl.ds(part * WIDE, WIDE))
+        for i in range(WIDE // TC):
+            k1[part * (WIDE // TC) + i] = total[:, i * TC : (i + 1) * TC]
 
     for j in range(NT):
         arrived(r1.at[j], RS + 3 * j)
@@ -343,6 +406,20 @@
 
     for copy in sent:
         copy.wait_send()
+    for u in range(2):
+        for h in range(2):
+            up_message(u, 0, h).wait_send()
+
+        @pl.when(g == 1)
+        def _():
+            for h in range(2):
+                up_message(u, 1, h).wait_send()
+
+        @pl.when(relays)
+        def _():
+            for q in range(2):
+                up_relay(u, q).wait_send()
+
     for part in range(2):
         for h in range(2):
 
@@ -402,6 +479,7 @@
             pltpu.SemaphoreType.DMA((N_MSG,)),
             pltpu.SemaphoreType.DMA((N_MSG,)),
             pltpu.SemaphoreType.DMA((4,)),
+            pltpu.SemaphoreType.REGULAR,
         ],
         compiler_params=pltpu.CompilerParams(
             collective_id=0, has_side_effects=True, vmem_limit_bytes=16 * 1024 * 1024

time: 77.1 us -> 77.2 us (level)
  no operation moved by 1% of the time
where the time goes in v4:
time: 77.2 us; the launch traced here: 76.9 us
  Pallas kernels  76.2 us (99%)
    pallas_call x1, Pallas kernels, per_device(): pl.pallas_call(kernel, out_shape=(jax.ShapeDtypeStruct((D, UNITS), BF16),...  74.9 us

profile of v4, /device:TPU:1, one launch (start us, length us, event | category | flops | bytes accessed | tf_op | source)
XLA Modules:
  0.0 76.9 jit_solution(6226683382982159531)
XLA Ops:
  0.6 74.9 %handoff.1 = (bf16[2048,256]{1,0:T(8,128)(2,1)S(1)}, bf16[256,2048]{1,0:T(8,128)(2,1)S(1)}, bf16[64,512]{1,0:T(8,128)(2,1)S(1)}) custom-call(bf16[512,2048]{1,0:T(8,128)(2,1)} %tok_hbm.1, f32[1,64]{1,0:T(1,128)} %bitcast.2, f32[64,512]{1,0:T(8,128)} %upw_hbm.1, f32[256,128]{1,0:T(8,128)} %dnw_hbm.1), custom_call_target="tpu_custom_call" | custom-call | tf_op jit(solution)/shard_map/handoff/pallas_call | solution.py:452
  75.5 1.3 %write_out.1 = (bf16[2048,256]{1,0:T(8,128)(2,1)}, bf16[256,2048]{1,0:T(8,128)(2,1)}, bf16[64,512]{1,0:T(8,128)(2,1)}) custom-call(bf16[2048,256]{1,0:T(8,128)(2,1)S(1)} %get-tuple-element.9.up_ref, bf16[256,2048]{1,0:T(8,128)(2,1)S(1)} %get-tuple-element.10.dn_ref, bf16[64,512]{1,0:T(8,128)(2,1)S(1)} %get-tuple-element.11.mix_ref), custom_call_target="tpu_custom_call" | custom-call | tf_op jit(solution)/shard_map/write_out/pallas_call | solution.py:493

commit v5 on v4

--- a/solution.py
+++ b/solution.py
@@ -16,7 +16,6 @@
 NT = 4
 TC = TOK // NT
 NORM_U, NORM_A, NORM_B = 18, 24, 32
-WIDE = 256
 
 
 def numbered(*sizes):
@@ -27,9 +26,11 @@
     return (*firsts, at)
 
 
-UP1, UPF, UPX, UPC, DNG, DNX, DNC, DTY, DTX, DTC, HY, RS, N_MSG = numbered(
-    8, 4, 12, 16, 1, 6, 8, 8, 6, 8, 12, 3 * NT
+UP1, UPF, UPX, UPC, DNG, DNX, DNC, DTY, DTX, DTC, HY, RS, N_RECV = numbered(
+    4, 4, 12, 2, 1, 2, 1, 2, 6, 1, NT, 3 * NT
 )
+S_W, S_L, S_G, S_R, S_Y, S_X, N_SEND = numbered(1, 1, 1, 1, 1, 1)
+KIB = 1024
 
 
 def kernel(
@@ -51,24 +52,23 @@
     def dev(gg, zz, yy, xx, kk):
         return (gg, zz * 4 + yy, xx * 2 + kk)
 
-    def message(src, dst, i, to, j=None):
+    def message(src, dst, i, to, group):
         return pltpu.make_async_remote_copy(
-            src_ref=src, dst_ref=dst,
-            send_sem=ssem.at[i], recv_sem=rsem.at[i if j is None else j],
+            src_ref=src, dst_ref=dst, send_sem=ssem.at[group], recv_sem=rsem.at[i],
             device_id=to, device_id_type=MESH,
         )
 
-    sent = []
-
-    def send(src, dst, i, to, j=None):
-        copy = message(src, dst, i, to, j)
-        copy.start()
-        sent.append(copy)
+    def send(src, dst, i, to, group=S_W):
+        message(src, dst, i, to, group).start()
 
     to_core = dev(g, zl, y, x, ok)
 
-    def arrived(dst, i):
-        message(dst, dst, 0, to_core, i).wait_recv()
+    def arrived(landed, i):
+        message(landed, landed, i, to_core, S_W).wait_recv()
+
+    def all_left(group, size):
+        rows = nrm.at[pl.ds(0, size // (2 * D)), :]
+        message(rows, rows, 0, to_core, group).wait_send()
 
     steps = (2, 1, 3)
     x_to = [dev(g, zl, y, (x + s) % 4, k) for s in steps]
@@ -156,14 +156,12 @@
         start = ((a_of(xx) + 4 * q) * 4 + 2 * (1 - kk)) * 64
         return up_buf.at[pl.ds(pl.multiple_of(start, 128), 128), pl.ds(u * HALF, HALF)]
 
-    j_me = b2 * 2 + y % 2
-
     def up_message(u, gg, h):
         xx = (x + zl + h + 2 * gg) % 4
         to = (gg, (4 * g + x) * 4 + 2 * k + h, xx * 2 + (1 - y // 2))
         slot = up_buf.at[pl.ds(pl.multiple_of(f * 64, 64), 64), pl.ds(u * HALF, HALF)]
         src = u_send.at[h, :, pl.ds(u * HALF, HALF)]
-        return message(src, slot, UP1 + u * 4 + gg * 2 + h, to, UP1 + u * 4 + j_me)
+        return message(src, slot, UP1 + u * 2 + b2, to, (S_W, S_G)[gg])
 
     def up_first(u):
         for h in range(2):
@@ -176,7 +174,7 @@
 
     def up_relay(u, q):
         piece = up_piece(x, q, k, u)
-        return message(piece, piece, UPF + u * 2 + q, to_gr)
+        return message(piece, piece, UPF + u * 2 + q, to_gr, S_R)
 
     up_first(0)
 
@@ -192,7 +190,7 @@
     def dt_to_y(part, h):
         return message(
             dt_send.at[part, h], dt_buf.at[y, dt_rows(part, x), :],
-            DTY + part * 4 + h, dev(g, zl, 2 * k + h, x, k), DTY + part * 4 + y,
+            DTY + part, dev(g, zl, 2 * k + h, x, k), S_Y,
         )
 
     def dt_over_y(part):
@@ -208,25 +206,20 @@
 
     def dt_from_x(part):
         piece = dt_piece(part, x)
-        return [message(piece, piece, DTX + part * 3 + d, x_to[d]) for d in range(3)] + [
-            message(piece, piece, DTC + part * 4, to_core)
+        return [message(piece, piece, DTX + part * 3 + d, x_to[d], S_X) for d in range(3)] + [
+            message(piece, piece, DTC, to_core, S_X)
         ]
 
     def dt_over_x(part):
         @pl.when(owner)
         def _():
-            for src in range(4):
-
-                @pl.when(y != src)
-                def _():
-                    arrived(dt_buf.at[src, dt_rows(part, x), :], DTY + part * 4 + src)
-
+            arrived(dt_buf.at[pl.ds(0, 3), dt_rows(part, x), :], DTY + part)
             for copy in dt_from_x(part):
                 copy.start()
 
     def dt_to_core(part, d):
         piece = dt_piece(part, x_from[d])
-        return message(piece, piece, DTC + part * 4 + 1 + d, to_core)
+        return message(piece, piece, DTC, to_core, S_X)
 
     def dt_over_core(part):
         @pl.when(owner)
@@ -238,14 +231,14 @@
     def dn_over_x(part):
         piece = dn_piece(halves[part], x, k)
         for d in range(3):
-            send(piece, piece, DNX + part * 3 + d, x_to[d])
-        send(piece, piece, DNC + part * 4, to_core)
+            send(piece, piece, DNX + part, x_to[d])
+        send(piece, piece, DNC, to_core)
 
     def dn_over_core(part):
-        for d in (1, 2, 0):
+        arrived(dn_buf.at[:, pl.ds(0, 3 * 128)], DNX + part)
+        for d in range(3):
             piece = dn_piece(halves[part], x_from[d], k)
-            arrived(piece, DNX + part * 3 + d)
-            send(piece, piece, DNC + part * 4 + 1 + d, to_core)
+            send(piece, piece, DNC, to_core)
 
     dt_over_y(0)
     dn_over_x(0)
@@ -279,10 +272,7 @@
 
             @pl.when(jnp.logical_not(relayed))
             def _():
-                for w in range(2):
-                    start = ((a_me + 4 * q) * 4 + 2 * ok + w) * 64
-                    slot = up_buf.at[pl.ds(pl.multiple_of(start, 64), 64), pl.ds(u * HALF, HALF)]
-                    arrived(slot, UP1 + u * 4 + q * 2 + w)
+                arrived(up_piece(x, q, k, u), UP1 + u * 2 + q)
 
             @pl.when(relays)
             def _():
@@ -291,7 +281,7 @@
             piece = up_piece(x, q, k, u)
             for d in range(3):
                 send(piece, piece, UPX + u * 6 + q * 3 + d, x_to[d])
-            send(piece, piece, UPC + u * 8 + q * 4, to_core)
+            send(piece, piece, UPC + u, to_core)
 
     send(dn_piece(g, x, k), dn_piece(g, x, k), DNG, to_gr)
     up_in(0)
@@ -302,28 +292,23 @@
             for q in range(2):
                 piece = up_piece(x_from[d], q, k, u)
                 arrived(piece, UPX + u * 6 + q * 3 + d)
-                send(piece, piece, UPC + u * 8 + q * 4 + 1 + d, to_core)
-
-    def hidden_out(u, part):
-        piece = h_buf.at[y, pl.ds(part * WIDE, WIDE), pl.ds(u * HALF, HALF)]
+                send(piece, piece, UPC + u, to_core)
+
+    def hidden_out(u, j):
+        piece = h_buf.at[y, pl.ds(j * TC, TC), pl.ds(u * HALF, HALF)]
         for d in range(3):
-            send(piece, piece, HY + u * 6 + part * 3 + d, y_to[d])
-
-    def hidden_half(u):
-        for q in range(2):
-            arrived(up_piece(x, q, ok, u), UPC + u * 8 + q * 4)
-            for d in range(3):
-                arrived(up_piece(x_from[d], q, ok, u), UPC + u * 8 + q * 4 + 1 + d)
+            send(piece, piece, HY + j, y_to[d], S_L)
+
+    def hidden_half(u, order):
+        arrived(up_buf.at[pl.ds(0, D // 2), pl.ds(u * HALF, HALF)], UPC + u)
         units = pl.ds(u * HALF, HALF)
         for part in range(2):
-            at = pl.ds(part * WIDE, WIDE)
+            at = pl.ds(part * TOK // 2, TOK // 2)
             pre = jnp.dot(nrm[at, :], up_buf[:, units], preferred_element_type=F32)
             pre = jnp.maximum(pre, 0.0)
             h_buf[y, at, units] = (pre * pre).astype(BF16)
-            if (u, part) != (0, 1):
-                hidden_out(u, part)
-            if (u, part) == (1, 0):
-                hidden_out(0, 1)
+            for uu, j in order[part]:
+                hidden_out(uu, j)
 
     dt_over_core(0)
     up_to_core(0)
@@ -333,11 +318,11 @@
         dt_send[1, h] = dt_other[h * 64 : (h + 1) * 64]
     dt_over_y(1)
 
-    hidden_half(0)
+    hidden_half(0, (((0, 0), (0, 1)), ((0, 2),)))
 
     dt_over_x(1)
     up_to_core(1)
-    hidden_half(1)
+    hidden_half(1, (((1, 0), (1, 1)), ((1, 2), (0, 3), (1, 3))))
 
     dn_over_x(1)
 
@@ -345,17 +330,14 @@
 
     @pl.when(jnp.logical_not(owner))
     def _():
-        for part in range(2):
-            arrived(dt_piece(part, x), DTC + part * 4)
-            for d in range(3):
-                arrived(dt_piece(part, x_from[d]), DTC + part * 4 + 1 + d)
-
-    def times_hidden(first, at):
+        arrived(dt_buf, DTC)
+
+    def times_hidden(first, j):
         rows_at = pl.ds(pl.multiple_of(first, 256), 256)
-        total = jnp.zeros((256, WIDE), F32)
+        total = jnp.zeros((256, TC), F32)
         for yy in range(4):
             total += lax.dot_general(
-                dt_buf[yy, rows_at, :], h_buf[yy, at, :],
+                dt_buf[yy, rows_at, :], h_buf[yy, pl.ds(j * TC, TC), :],
                 (((1,), (1,)), ((), ())), preferred_element_type=F32,
             )
         return total
@@ -363,76 +345,60 @@
     def aligned(start, size):
         return pl.ds(pl.multiple_of(start, 64), size)
 
-    for part in range(2):
-        at = pl.ds(part * WIDE, WIDE)
-        for u in range(2):
-            for d in range(3):
-                piece = h_buf.at[y_from[d], at, pl.ds(u * HALF, HALF)]
-                arrived(piece, HY + u * 6 + part * 3 + d)
-        total = times_hidden((1 - b0) * 256, at).astype(BF16)
-        for i in range(WIDE // TC):
-            j = part * (WIDE // TC) + i
-            s1[j] = total[:, i * TC : (i + 1) * TC]
-            send(s1.at[j], r1.at[j], RS + 3 * j, to_z1)
-    for part in range(2):
-        total = times_hidden(b0 * 256, pl.ds(part * WIDE, WIDE))
-        for i in range(WIDE // TC):
-            k1[part * (WIDE // TC) + i] = total[:, i * TC : (i + 1) * TC]
-
-    for j in range(NT):
+    def second_matmul(j):
+        arrived(h_buf.at[pl.ds(0, 3), pl.ds(0, TC), :], HY + j)
+        s1[j] = times_hidden((1 - b0) * 256, j).astype(BF16)
+        send(s1.at[j], r1.at[j], RS + 3 * j, to_z1, S_L)
+        k1[j] = times_hidden(b0 * 256, j)
+
+    def halve(j):
         arrived(r1.at[j], RS + 3 * j)
         out, keep = aligned((1 - b1) * 128, 128), aligned(b1 * 128, 128)
         s2[j] = (k1[j, out, :] + r1[j, out, :].astype(F32)).astype(BF16)
-        send(s2.at[j], r2.at[j], RS + 3 * j + 1, to_z2)
+        send(s2.at[j], r2.at[j], RS + 3 * j + 1, to_z2, S_L)
         k2[j] = k1[j, keep, :] + r1[j, keep, :].astype(F32)
+
+    for j in range(NT):
+        second_matmul(j)
+        if j >= 2:
+            halve(j - 2)
+    halve(NT - 2)
+    halve(NT - 1)
     for j in range(NT):
         arrived(r2.at[j], RS + 3 * j + 1)
         out, keep = aligned((1 - b2) * 64, 64), aligned(b2 * 64, 64)
         s3[j] = (k2[j, out, :] + r2[j, out, :].astype(F32)).astype(BF16)
-        send(s3.at[j], r3.at[j], RS + 3 * j + 2, to_z4)
+        send(s3.at[j], r3.at[j], RS + 3 * j + 2, to_z4, S_L)
         k3[j] = k2[j, keep, :] + r2[j, keep, :].astype(F32)
 
     dn_over_core(0)
     dn_over_core(1)
 
-    for part in range(2):
-        arrived(dn_piece(halves[part], x, ok), DNC + part * 4)
-        for d in range(3):
-            arrived(dn_piece(halves[part], x_from[d], ok), DNC + part * 4 + 1 + d)
+    arrived(dn_buf.at[:, pl.ds(0, D // 2)], DNC)
 
     for j in range(NT):
         arrived(r3.at[j], RS + 3 * j + 2)
         mix_ref[:, j * TC : (j + 1) * TC] = (k3[j] + r3[j].astype(F32)).astype(BF16)
 
-    for copy in sent:
-        copy.wait_send()
-    for u in range(2):
-        for h in range(2):
-            up_message(u, 0, h).wait_send()
-
-        @pl.when(g == 1)
-        def _():
-            for h in range(2):
-                up_message(u, 1, h).wait_send()
-
-        @pl.when(relays)
-        def _():
-            for q in range(2):
-                up_relay(u, q).wait_send()
-
-    for part in range(2):
-        for h in range(2):
-
-            @pl.when(2 * k + h != y)
-            def _():
-                dt_to_y(part, h).wait_send()
-
-        @pl.when(owner)
-        def _():
-            for copy in dt_from_x(part):
-                copy.wait_send()
-            for d in range(3):
-                dt_to_core(part, d).wait_send()
+    all_left(S_W, (64 + 384 + 512 + 64 + 384 + 512) * KIB)
+    all_left(S_L, (768 + 256 + 128 + 64) * KIB)
+
+    @pl.when(g == 1)
+    def _():
+        all_left(S_G, 64 * KIB)
+
+    @pl.when(relays)
+    def _():
+        all_left(S_R, 128 * KIB)
+
+    @pl.when(owner)
+    def _():
+        all_left(S_Y, 64 * KIB)
+        all_left(S_X, 2 * 7 * 128 * KIB)
+
+    @pl.when(jnp.logical_not(owner))
+    def _():
+        all_left(S_Y, 128 * KIB)
 
 
 def write_out(up_ref, dn_ref, mix_ref, up_hbm, dn_hbm, mix_hbm, lsem):
@@ -476,8 +442,8 @@
             pltpu.VMEM((NT, 64, TC), BF16),
             pltpu.VMEM((NT, 64, TC), BF16),
             pltpu.VMEM((NT, 64, TC), F32),
-            pltpu.SemaphoreType.DMA((N_MSG,)),
-            pltpu.SemaphoreType.DMA((N_MSG,)),
+            pltpu.SemaphoreType.DMA((N_SEND,)),
+            pltpu.SemaphoreType.DMA((N_RECV,)),
             pltpu.SemaphoreType.DMA((4,)),
             pltpu.SemaphoreType.REGULAR,
         ],

time: 77.2 us -> 74.8 us (0.969)
  Pallas kernels: 76.2 us -> 74 us
    pallas_call x1, Pallas kernels: 74.9 us -> 72.7 us  [per_device(): pl.pallas_call(kernel, out_shape=(jax.ShapeDtypeStruct((D, UNITS), BF16),...]
where the time goes in v5:
time: 74.8 us; the launch traced here: 74.7 us
  Pallas kernels  74 us (99%)
    pallas_call x1, Pallas kernels, per_device(): pl.pallas_call(kernel, out_shape=(jax.ShapeDtypeStruct((D, UNITS), BF16),...  72.7 us

profile of v5, /device:TPU:1, one launch (start us, length us, event | category | flops | bytes accessed | tf_op | source)
XLA Modules:
  0.0 74.7 jit_solution(15474057679622455246)
XLA Ops:
  0.6 72.7 %handoff.1 = (bf16[2048,256]{1,0:T(8,128)(2,1)S(1)}, bf16[256,2048]{1,0:T(8,128)(2,1)S(1)}, bf16[64,512]{1,0:T(8,128)(2,1)S(1)}) custom-call(bf16[512,2048]{1,0:T(8,128)(2,1)} %tok_hbm.1, f32[1,64]{1,0:T(1,128)} %bitcast.2, f32[64,512]{1,0:T(8,128)} %upw_hbm.1, f32[256,128]{1,0:T(8,128)} %dnw_hbm.1), custom_call_target="tpu_custom_call" | custom-call | tf_op jit(solution)/shard_map/handoff/pallas_call | solution.py:418
  73.3 1.3 %write_out.1 = (bf16[2048,256]{1,0:T(8,128)(2,1)}, bf16[256,2048]{1,0:T(8,128)(2,1)}, bf16[64,512]{1,0:T(8,128)(2,1)}) custom-call(bf16[2048,256]{1,0:T(8,128)(2,1)S(1)} %get-tuple-element.9.up_ref, bf16[256,2048]{1,0:T(8,128)(2,1)S(1)} %get-tuple-element.10.dn_ref, bf16[64,512]{1,0:T(8,128)(2,1)S(1)} %get-tuple-element.11.mix_ref), custom_call_target="tpu_custom_call" | custom-call | tf_op jit(solution)/shard_map/write_out/pallas_call | solution.py:459

commit v6 on v5

--- a/solution.py
+++ b/solution.py
@@ -15,6 +15,7 @@
 HALF = 128
 NT = 4
 TC = TOK // NT
+STEPS = (3, 3, 2, 2)
 NORM_U, NORM_A, NORM_B = 18, 24, 32
 
 
@@ -31,6 +32,7 @@
 )
 S_W, S_L, S_G, S_R, S_Y, S_X, N_SEND = numbered(1, 1, 1, 1, 1, 1)
 KIB = 1024
+MATES = tuple(range(1, 8)) if 1 in STEPS else (1, 2, 4, 6) if 2 in STEPS else (1, 2, 4)
 
 
 def kernel(
@@ -39,6 +41,7 @@
     gain_ref, upw_ref, dnw_ref,
     u_send, dt_send, dt_buf, nrm, h_buf,
     s1, r1, k1, s2, r2, k2, s3, r3, k3,
+    sm, rm, sd, rd, kd,
     ssem, rsem, lsem, far_sem,
 ):
     g = lax.axis_index("gr")
@@ -81,6 +84,13 @@
     to_z4 = dev(g, zl + 4 - 8 * b2, y, x, k)
     to_gr = dev(og, zl, y, x, k)
 
+    place = b0 * 4 + b1 * 2 + b2
+
+    def z_mate(m):
+        flip = [abs(b - (m >> i) % 2) for i, b in enumerate((b0, b1, b2))]
+        return dev(g, flip[0] + 2 * flip[1] + 4 * flip[2], y, x, k), flip[0] * 4 + flip[1] * 2 + flip[2]
+
+
     xs, ks, hs = zl % 4, y // 2, y % 2
     relayed = jnp.logical_and(g == 1, b2 == 0)
     relays = jnp.logical_and(g == 0, b2 == 0)
@@ -107,7 +117,7 @@
     def _():
         greet(to_gr)
 
-    for who in (*x_to, *y_to, to_z1, to_z2, to_z4, to_core):
+    for who in (*x_to, *y_to, to_core, *(z_mate(m)[0] for m in MATES)):
         greet(who)
 
     loads = [
@@ -144,11 +154,11 @@
 
     @pl.when(g == 0)
     def _():
-        pl.semaphore_wait(barrier, 12)
+        pl.semaphore_wait(barrier, 9 + len(MATES))
 
     @pl.when(g == 1)
     def _():
-        pl.semaphore_wait(barrier, 15)
+        pl.semaphore_wait(barrier, 12 + len(MATES))
         pl.semaphore_signal(far_sem, inc=1, device_id=to_gr, device_id_type=MESH)
 
 
@@ -358,13 +368,46 @@
         send(s2.at[j], r2.at[j], RS + 3 * j + 1, to_z2, S_L)
         k2[j] = k1[j, keep, :] + r1[j, keep, :].astype(F32)
 
+    def halve_and_send(j):
+        arrived(r1.at[j], RS + 3 * j)
+        half_place = b1 * 2 + b2
+        for m in (6, 4, 2):
+            to, at_place = z_mate(m)
+            at = at_place % 4
+            rows_at = aligned(at * 64, 64)
+            sm[j, at] = (k1[j, rows_at, :] + r1[j, rows_at, :].astype(F32)).astype(BF16)
+            send(sm.at[j, at], rm.at[j, half_place], RS + 3 * j + 1, to, S_L)
+        keep = aligned(half_place * 64, 64)
+        k3[j] = k1[j, keep, :] + r1[j, keep, :].astype(F32)
+
+    def second_matmul_to_all(j):
+        arrived(h_buf.at[pl.ds(0, 3), pl.ds(0, TC), :], HY + j)
+        sd[pl.ds((1 - b0) * 4, 4)] = times_hidden((1 - b0) * 256, j).astype(BF16).reshape(4, 64, TC)
+        for m in (7, 5, 3, 1):
+            to, at = z_mate(m)
+            send(sd.at[at], rd.at[place], RS + 3 * j, to, S_L)
+        kd[...] = times_hidden(b0 * 256, j).reshape(4, 64, TC)
+        for m in (6, 4, 2):
+            to, at = z_mate(m)
+            sd[at] = kd[at % 4].astype(BF16)
+            send(sd.at[at], rd.at[place], RS + 3 * j, to, S_L)
+
+    def next_step(j):
+        if STEPS[j] == 3:
+            halve(j)
+        elif STEPS[j] == 2:
+            halve_and_send(j)
+
     for j in range(NT):
-        second_matmul(j)
+        if STEPS[j] == 1:
+            second_matmul_to_all(j)
+        else:
+            second_matmul(j)
         if j >= 2:
-            halve(j - 2)
-    halve(NT - 2)
-    halve(NT - 1)
-    for j in range(NT):
+            next_step(j - 2)
+    next_step(NT - 2)
+    next_step(NT - 1)
+    for j in [j for j in range(NT) if STEPS[j] == 3]:
         arrived(r2.at[j], RS + 3 * j + 1)
         out, keep = aligned((1 - b2) * 64, 64), aligned(b2 * 64, 64)
         s3[j] = (k2[j, out, :] + r2[j, out, :].astype(F32)).astype(BF16)
@@ -377,11 +420,23 @@
     arrived(dn_buf.at[:, pl.ds(0, D // 2)], DNC)
 
     for j in range(NT):
-        arrived(r3.at[j], RS + 3 * j + 2)
-        mix_ref[:, j * TC : (j + 1) * TC] = (k3[j] + r3[j].astype(F32)).astype(BF16)
+        if STEPS[j] == 3:
+            arrived(r3.at[j], RS + 3 * j + 2)
+            total = k3[j] + r3[j].astype(F32)
+        elif STEPS[j] == 2:
+            arrived(rm.at[j, pl.ds(0, 3)], RS + 3 * j + 1)
+            total = k3[j]
+            for m in (2, 4, 6):
+                total += rm[j, z_mate(m)[1] % 4].astype(F32)
+        else:
+            arrived(rd.at[pl.ds(0, 7)], RS + 3 * j)
+            total = kd[place % 4]
+            for m in range(1, 8):
+                total += rd[z_mate(m)[1]].astype(F32)
+        mix_ref[:, j * TC : (j + 1) * TC] = total.astype(BF16)
 
     all_left(S_W, (64 + 384 + 512 + 64 + 384 + 512) * KIB)
-    all_left(S_L, (768 + 256 + 128 + 64) * KIB)
+    all_left(S_L, (768 + NT * 112) * KIB)
 
     @pl.when(g == 1)
     def _():
@@ -442,6 +497,11 @@
             pltpu.VMEM((NT, 64, TC), BF16),
             pltpu.VMEM((NT, 64, TC), BF16),
             pltpu.VMEM((NT, 64, TC), F32),
+            pltpu.VMEM((NT, 4, 64, TC), BF16),
+            pltpu.VMEM((NT, 4, 64, TC), BF16),
+            pltpu.VMEM((8, 64, TC), BF16),
+            pltpu.VMEM((8, 64, TC), BF16),
+            pltpu.VMEM((4, 64, TC), F32),
             pltpu.SemaphoreType.DMA((N_SEND,)),
             pltpu.SemaphoreType.DMA((N_RECV,)),
             pltpu.SemaphoreType.DMA((4,)),

time: 74.8 us -> 72.5 us (0.969)
  Pallas kernels: 74 us -> 71.7 us
    pallas_call x1, Pallas kernels: 72.7 us -> 70.4 us  [per_device(): pl.pallas_call(kernel, out_shape=(jax.ShapeDtypeStruct((D, UNITS), BF16),...]
where the time goes in v6:
time: 72.5 us; the launch traced here: 72.4 us
  Pallas kernels  71.7 us (99%)
    pallas_call x1, Pallas kernels, per_device(): pl.pallas_call(kernel, out_shape=(jax.ShapeDtypeStruct((D, UNITS), BF16),...  70.4 us

profile of v6, /device:TPU:1, one launch (start us, length us, event | category | flops | bytes accessed | tf_op | source)
XLA Modules:
  0.0 72.4 jit_solution(13884981837389081838)
XLA Ops:
  0.6 70.4 %handoff.1 = (bf16[2048,256]{1,0:T(8,128)(2,1)S(1)}, bf16[256,2048]{1,0:T(8,128)(2,1)S(1)}, bf16[64,512]{1,0:T(8,128)(2,1)S(1)}) custom-call(bf16[512,2048]{1,0:T(8,128)(2,1)} %tok_hbm.1, f32[1,64]{1,0:T(1,128)} %bitcast.2, f32[64,512]{1,0:T(8,128)} %upw_hbm.1, f32[256,128]{1,0:T(8,128)} %dnw_hbm.1), custom_call_target="tpu_custom_call" | custom-call | tf_op jit(solution)/shard_map/handoff/pallas_call | solution.py:473
  71.0 1.3 %write_out.1 = (bf16[2048,256]{1,0:T(8,128)(2,1)}, bf16[256,2048]{1,0:T(8,128)(2,1)}, bf16[64,512]{1,0:T(8,128)(2,1)}) custom-call(bf16[2048,256]{1,0:T(8,128)(2,1)S(1)} %get-tuple-element.9.up_ref, bf16[256,2048]{1,0:T(8,128)(2,1)S(1)} %get-tuple-element.10.dn_ref, bf16[64,512]{1,0:T(8,128)(2,1)S(1)} %get-tuple-element.11.mix_ref), custom_call_target="tpu_custom_call" | custom-call | tf_op jit(solution)/shard_map/write_out/pallas_call | solution.py:519

commit v7 on v6

--- a/solution.py
+++ b/solution.py
@@ -289,7 +289,7 @@
                 up_relay(u, q).start()
 
             piece = up_piece(x, q, k, u)
-            for d in range(3):
+            for d in (1, 2, 0):
                 send(piece, piece, UPX + u * 6 + q * 3 + d, x_to[d])
             send(piece, piece, UPC + u, to_core)
 
@@ -306,7 +306,7 @@
 
     def hidden_out(u, j):
         piece = h_buf.at[y, pl.ds(j * TC, TC), pl.ds(u * HALF, HALF)]
-        for d in range(3):
+        for d in (1, 2, 0):
             send(piece, piece, HY + j, y_to[d], S_L)
 
     def hidden_half(u, order):

time: 72.5 us -> 72 us (level)
  no operation moved by 1% of the time
where the time goes in v7:
time: 72 us; the launch traced here: 71.8 us
  Pallas kernels  71.2 us (99%)
    pallas_call x1, Pallas kernels, per_device(): pl.pallas_call(kernel, out_shape=(jax.ShapeDtypeStruct((D, UNITS), BF16),...  69.9 us

profile of v7, /device:TPU:1, one launch (start us, length us, event | category | flops | bytes accessed | tf_op | source)
XLA Modules:
  0.0 71.8 jit_solution(15783021561135314579)
XLA Ops:
  0.6 69.9 %handoff.1 = (bf16[2048,256]{1,0:T(8,128)(2,1)S(1)}, bf16[256,2048]{1,0:T(8,128)(2,1)S(1)}, bf16[64,512]{1,0:T(8,128)(2,1)S(1)}) custom-call(bf16[512,2048]{1,0:T(8,128)(2,1)} %tok_hbm.1, f32[1,64]{1,0:T(1,128)} %bitcast.2, f32[64,512]{1,0:T(8,128)} %upw_hbm.1, f32[256,128]{1,0:T(8,128)} %dnw_hbm.1), custom_call_target="tpu_custom_call" | custom-call | tf_op jit(solution)/shard_map/handoff/pallas_call | solution.py:473
  70.5 1.3 %write_out.1 = (bf16[2048,256]{1,0:T(8,128)(2,1)}, bf16[256,2048]{1,0:T(8,128)(2,1)}, bf16[64,512]{1,0:T(8,128)(2,1)}) custom-call(bf16[2048,256]{1,0:T(8,128)(2,1)S(1)} %get-tuple-element.9.up_ref, bf16[256,2048]{1,0:T(8,128)(2,1)S(1)} %get-tuple-element.10.dn_ref, bf16[64,512]{1,0:T(8,128)(2,1)S(1)} %get-tuple-element.11.mix_ref), custom_call_target="tpu_custom_call" | custom-call | tf_op jit(solution)/shard_map/write_out/pallas_call | solution.py:519

commit v8 on v7

--- a/solution.py
+++ b/solution.py
@@ -216,7 +216,7 @@
 
     def dt_from_x(part):
         piece = dt_piece(part, x)
-        return [message(piece, piece, DTX + part * 3 + d, x_to[d], S_X) for d in range(3)] + [
+        return [message(piece, piece, DTX + part * 3 + d, x_to[d], S_X) for d in (1, 2, 0)] + [
             message(piece, piece, DTC, to_core, S_X)
         ]
 
@@ -240,7 +240,7 @@
 
     def dn_over_x(part):
         piece = dn_piece(halves[part], x, k)
-        for d in range(3):
+        for d in (1, 2, 0):
             send(piece, piece, DNX + part, x_to[d])
         send(piece, piece, DNC, to_core)
 

time: 72 us -> 73.9 us (1.026)
  Pallas kernels: 71.2 us -> 73.1 us
    pallas_call x1, Pallas kernels: 69.9 us -> 71.7 us  [per_device(): pl.pallas_call(kernel, out_shape=(jax.ShapeDtypeStruct((D, UNITS), BF16),...]
where the time goes in v8:
time: 73.9 us; the launch traced here: 73.7 us
  Pallas kernels  73.1 us (99%)
    pallas_call x1, Pallas kernels, per_device(): pl.pallas_call(kernel, out_shape=(jax.ShapeDtypeStruct((D, UNITS), BF16),...  71.7 us

profile of v8, /device:TPU:1, one launch (start us, length us, event | category | flops | bytes accessed | tf_op | source)
XLA Modules:
  0.0 73.7 jit_solution(2413526638001957298)
XLA Ops:
  0.6 71.7 %handoff.1 = (bf16[2048,256]{1,0:T(8,128)(2,1)S(1)}, bf16[256,2048]{1,0:T(8,128)(2,1)S(1)}, bf16[64,512]{1,0:T(8,128)(2,1)S(1)}) custom-call(bf16[512,2048]{1,0:T(8,128)(2,1)} %tok_hbm.1, f32[1,64]{1,0:T(1,128)} %bitcast.2, f32[64,512]{1,0:T(8,128)} %upw_hbm.1, f32[256,128]{1,0:T(8,128)} %dnw_hbm.1), custom_call_target="tpu_custom_call" | custom-call | tf_op jit(solution)/shard_map/handoff/pallas_call | solution.py:473
  72.4 1.3 %write_out.1 = (bf16[2048,256]{1,0:T(8,128)(2,1)}, bf16[256,2048]{1,0:T(8,128)(2,1)}, bf16[64,512]{1,0:T(8,128)(2,1)}) custom-call(bf16[2048,256]{1,0:T(8,128)(2,1)S(1)} %get-tuple-element.9.up_ref, bf16[256,2048]{1,0:T(8,128)(2,1)S(1)} %get-tuple-element.10.dn_ref, bf16[64,512]{1,0:T(8,128)(2,1)S(1)} %get-tuple-element.11.mix_ref), custom_call_target="tpu_custom_call" | custom-call | tf_op jit(solution)/shard_map/write_out/pallas_call | solution.py:519
